TPU v7x, 128 devices: a whole 4x4x4 slice. The times are simulated.
128 devices in a mesh: rep: 4 (over x), fs: 2 (over core), tp: 16 (over z, y).
Axes of the slice: x: 4, y: 4, z: 4, core: 2. Of those that a mesh axis runs over, the one named last changes fastest.
Arguments:
- layer_input: bfloat16 [10240, 2048], P(('rep', 'fs'), 'tp'), may hold values from -6 to 6
- cotangent: bfloat16 [10240, 2048], P(('rep', 'fs'), 'tp'), may hold values from -8 to 8
- gate_pre: bfloat16 [10240, 3072], P('rep', 'fs'), may hold values from -8 to 8
- up_pre: bfloat16 [10240, 3072], P('rep', 'fs'), may hold values from -6 to 6
- gate_weight: bfloat16 [2048, 3072], P('tp', 'fs'), may hold values from -0.125 to 0.125
- up_weight: bfloat16 [2048, 3072], P('tp', 'fs'), may hold values from -0.125 to 0.125
- down_weight: bfloat16 [3072, 2048], P('fs', 'tp'), may hold values from -0.109375 to 0.109375
Outputs:
- input_grad: bfloat16 [10240, 2048], P(('rep', 'fs'), 'tp')
- gate_grad: float32 [2048, 3072], P('tp', 'fs')
- up_grad: float32 [2048, 3072], P('tp', 'fs')
- down_grad: float32 [3072, 2048], P('fs', 'tp')
- gate_rows_sq: float32 [2048], P('tp')
- up_rows_sq: float32 [2048], P('tp')
- down_rows_sq: float32 [3072], P('fs')
All inputs are finite; a program needn't handle non-finite values.
Results may differ from a plain program's by a relative error of at most 0.019.
Values may be sent and summed in bfloat16 or wider, within the bound.
A program may use at most 128 MiB of HBM per device.

v0:
```python
import math

import jax
import jax.numpy as jnp
from jax import lax
from jax.sharding import PartitionSpec as P


def gathered_total(x, axis):
    tiles = lax.all_gather(x, axis)
    return tiles.sum(axis=0)


def copy_for_each(x, axis):
    copies = jnp.broadcast_to(x, (lax.axis_size(axis), *x.shape))
    return lax.all_to_all(copies, axis, split_axis=0, concat_axis=0, tiled=True)


def taken_together(x, axis):
    return copy_for_each(x, axis).sum(axis=0)


def joined_along(tiles, dim):
    tiles = jnp.moveaxis(tiles, 0, dim)
    dims = tiles.shape
    return tiles.reshape(*dims[:dim], dims[dim] * dims[dim + 1], *dims[dim + 2 :])


def gather_packed(arrays, axis, dims):
    ravelled = jnp.concatenate([a.reshape(-1) for a in arrays])
    lines, at, gathered = (lax.all_gather(ravelled, axis), 0, [])
    for a, dim in zip(arrays, dims):
        tiles = lines[:, at : at + a.size].reshape(-1, *a.shape)
        gathered.append(joined_along(tiles, dim))
        at += a.size
    return tuple(gathered)


def sent_together(arrays, axis, dim, along):
    ends, at = ([], 0)
    for a in arrays[:-1]:
        at += a.shape[along]
        ends.append(at)
    both = jnp.concatenate(arrays, axis=along)
    return tuple(jnp.split(lax.all_gather(both, axis, axis=dim, tiled=True), ends, axis=along))


def over_copies(x, axis):
    everything = copy_for_each(x, axis)
    return jnp.sum(everything.astype(jnp.float32), axis=0)


def contract_rows(left_side, right_side):
    return lax.dot_general(
        left_side, right_side, (((0,), (0,)), ((), ())), preferred_element_type=jnp.float32
    )


def contract_cols(left_side, right_side):
    return lax.dot_general(
        left_side, right_side, (((1,), (1,)), ((), ())), preferred_element_type=jnp.float32
    )


def row_squares(gate_grad, up_grad, down_grad):
    gate_sq = jnp.sum(gate_grad * gate_grad, axis=1)
    up_sq = jnp.sum(up_grad * up_grad, axis=1)
    down_sq = jnp.sum(down_grad * down_grad, axis=1)
    gate_sq, up_sq = (gathered_total(gate_sq, "fs"), gathered_total(up_sq, "fs"))
    down_sq = taken_together(down_sq, "tp")
    return (gate_sq, up_sq, down_sq)


def on_device(layer_input, cotangent, gate_pre, up_pre, gate_weight, up_weight, down_weight):
    group_input, group_cotangent = gather_packed((layer_input, cotangent), "fs", (0, 0))
    full_cotangent, full_down = sent_together((group_cotangent, down_weight), "tp", 1, 0)
    hidden_grad = contract_cols(full_cotangent, full_down)
    gate_value = gate_pre.astype(jnp.float32)
    up_value = up_pre.astype(jnp.float32)
    sigmoid_gate = jax.nn.sigmoid(gate_value)
    activated = gate_value * sigmoid_gate
    hidden = (activated * up_value).astype(jnp.bfloat16)
    gate_delta = (
        hidden_grad * up_value * sigmoid_gate * (1.0 + gate_value * (1.0 - sigmoid_gate))
    ).astype(jnp.bfloat16)
    up_delta = (hidden_grad * activated).astype(jnp.bfloat16)
    input_grad = lax.psum_scatter(
        (contract_cols(gate_delta, gate_weight) + contract_cols(up_delta, up_weight)).astype(
            jnp.bfloat16
        ),
        "fs",
        scatter_dimension=0,
        tiled=True,
    )
    grad_scale = 1.0 / math.sqrt(group_input.shape[0] * lax.axis_size("rep"))
    gate_grad = contract_rows(group_input, gate_delta) * grad_scale
    up_grad = contract_rows(group_input, up_delta) * grad_scale
    down_grad = contract_rows(hidden, group_cotangent) * grad_scale
    gate_grad, up_grad, down_grad = (
        over_copies(gate_grad.astype(jnp.bfloat16), "rep").astype(jnp.float32),
        over_copies(up_grad.astype(jnp.bfloat16), "rep").astype(jnp.float32),
        over_copies(down_grad.astype(jnp.bfloat16), "rep").astype(jnp.float32),
    )
    gate_sq, up_sq, down_sq = row_squares(gate_grad, up_grad, down_grad)
    return (input_grad, gate_grad, up_grad, down_grad, gate_sq, up_sq, down_sq)


def solution(mesh):
    return jax.shard_map(
        on_device,
        mesh=mesh,
        in_specs=(
            P(("rep", "fs"), "tp"),
            P(("rep", "fs"), "tp"),
            P("rep", "fs"),
            P("rep", "fs"),
            P("tp", "fs"),
            P("tp", "fs"),
            P("fs", "tp"),
        ),
        out_specs=(
            P(("rep", "fs"), "tp"),
            P("tp", "fs"),
            P("tp", "fs"),
            P("fs", "tp"),
            P("tp"),
            P("tp"),
            P("fs"),
        ),
        check_vma=False,
    )
```

profile of v0, /device:TPU:1, one launch (start us, length us, event | category | flops | bytes accessed | tf_op | source)
XLA Modules:
  0.0 247.8 jit_solution(6285302619795963910)
XLA Ops:
  7.2 0.0 copy-start
  7.2 0.0 all-gather.10.cloned.1.call-start
  7.2 2.0 pad_maximum_fusion.1
  9.2 0.0 all-gather.10.cloned.1.call-update
  9.2 0.0 all-gather.8.cloned.1.call-start
  9.3 16.7 %all-gather.10.cloned.1.call-done = bf16[655360]{0:T(1024)(128)(2,1)} async-done(((bf16[327680]{0:T(1024)(128)(2,1)}), bf16[655360]{0:T(1024)(128)(2,1)}) %all-gather.10.cloned.1.call-update) | async-done | bytes 1310736 | tf_op jit(solution)/shard_map/all_gather | solution.py:31
  26.0 1.6 reshape.26
  27.6 1.0 fusion.23
  28.6 0.5 reshape_reshape.6
  29.1 2.0 pad_maximum_fusion
  31.1 0.0 all-gather.8.cloned.1.call-update
  31.1 8.6 %fusion.19 = bf16[1536,128]{1,0:T(8,128)(2,1)S(1)} fusion(bf16[2560,128]{1,0:T(8,128)(2,1)S(1)} %reshape_reshape.6, bf16[2560,1536]{1,0:T(8,128)(2,1)} %param.10, bf16[2560,1536]{1,0:T(8,128)(2,1)} %param.9), kind=kOutput, calls=%fused_computation.28 | convolution fusion | flops 1038483456 | bytes 16777216 | tf_op jit(solution)/shard_map/dot_general | solution.py:54
  39.7 1.4 broadcast_in_dim.14
  41.1 4.1 %all-to-all-start.2 = ((bf16[4,1536,128]{2,1,0:T(8,128)(2,1)}), bf16[4,1536,128]{2,1,0:T(8,128)(2,1)S(1)}, u32[]{:S(2)}, u32[]{:S(2)}) async-start(bf16[4,1536,128]{2,1,0:T(8,128)(2,1)} %broadcast_in_dim.14), calls=%async_computation.3 | async-start | bytes 3145728 | tf_op jit(solution)/shard_map/all_to_all | solution.py:16
  45.1 0.5 reshape_reshape.7
  45.6 19.8 %all-to-all-done.2 = bf16[4,1536,128]{2,1,0:T(8,128)(2,1)S(1)} async-done(((bf16[4,1536,128]{2,1,0:T(8,128)(2,1)}), bf16[4,1536,128]{2,1,0:T(8,128)(2,1)S(1)}, u32[]{:S(2)}, u32[]{:S(2)}) %all-to-all-start.2) | async-done | bytes 1572896 | tf_op jit(solution)/shard_map/all_to_all | solution.py:16
  65.4 0.2 convert_reduce_fusion
  65.7 0.0 copy-start.1
  65.7 0.9 copy-done.1
  66.6 0.3 multiply_reduce_fusion
  66.8 0.7 broadcast_in_dim.15
  67.5 6.7 %all-to-all-start.3 = ((f32[16,1,1536]{2,1,0:T(1,128)}), f32[16,1,1536]{2,1,0:T(1,128)S(1)}, u32[]{:S(2)}, u32[]{:S(2)}) async-start(f32[16,1,1536]{2,1,0:T(1,128)} %broadcast_in_dim.15), calls=%async_computation.4 | async-start | bytes 196608 | tf_op jit(solution)/shard_map/all_to_all | solution.py:16
  74.3 77.2 %all-gather.8.cloned.1.call-done = bf16[4096,2048]{1,0:T(8,128)(2,1)} async-done(((bf16[4096,128]{1,0:T(8,128)(2,1)}), bf16[4096,2048]{1,0:T(8,128)(2,1)}) %all-gather.8.cloned.1.call-update) | async-done | bytes 16777232 | tf_op jit(solution)/shard_map/all_gather | solution.py:45
  151.5 29.6 %multiply_convert_fusion = (bf16[2560,1536]{1,0:T(8,128)(2,1)}, bf16[2560,1536]{1,0:T(8,128)(2,1)}) fusion(bf16[2560,1536]{1,0:T(8,128)(2,1)} %param.9, bf16[2560,1536]{1,0:T(8,128)(2,1)} %param.10, bf16[4096,2048]{1,0:T(8,128)(2,1)} %all-gather.8.cloned.1.call-done), kind=kOutput, calls=%fused_computation.13 | convolution fusion | flops 16165109760 | bytes 48234496 | tf_op jit(solution)/shard_map/dot_general | solution.py:60
  181.1 4.5 %fusion.17 = bf16[128,1536]{1,0:T(8,128)(2,1)S(1)} fusion(bf16[2560,128]{1,0:T(8,128)(2,1)S(1)} %reshape_reshape.7, bf16[2560,1536]{1,0:T(8,128)(2,1)} %get-tuple-element.8), kind=kOutput, calls=%fused_computation.26 | convolution fusion | flops 1007026176 | bytes 8912896 | tf_op jit(solution)/shard_map/dot_general | solution.py:54
  185.5 0.0 all-to-all-done.3
  185.6 1.3 broadcast_in_dim.12
  186.8 3.6 %all-to-all-start = ((bf16[4,128,1536]{2,1,0:T(8,128)(2,1)}), bf16[4,128,1536]{2,1,0:T(8,128)(2,1)S(1)}, u32[]{:S(2)}, u32[]{:S(2)}) async-start(bf16[4,128,1536]{2,1,0:T(8,128)(2,1)} %broadcast_in_dim.12), calls=%async_computation.1 | async-start | bytes 3145728 | tf_op jit(solution)/shard_map/all_to_all | solution.py:16
  190.4 5.2 %fusion.18 = bf16[128,1536]{1,0:T(8,128)(2,1)} fusion(bf16[2560,128]{1,0:T(8,128)(2,1)S(1)} %reshape_reshape.7, bf16[2560,1536]{1,0:T(8,128)(2,1)} %get-tuple-element.7), kind=kOutput, calls=%fused_computation.27 | convolution fusion | flops 1007026176 | bytes 8912896 | tf_op jit(solution)/shard_map/dot_general | solution.py:54
  195.6 0.0 copy-done
  195.6 5.4 %fusion.24 = f32[2560,128]{1,0:T(8,128)S(1)} fusion(bf16[2560,1536]{1,0:T(8,128)(2,1)} %get-tuple-element.8, bf16[128,1536]{1,0:T(8,128)(2,1)S(1)} %copy-done), kind=kOutput, calls=%fused_computation.36 | convolution fusion | flops 1006632960 | bytes 9568256 | tf_op jit(solution)/shard_map/dot_general | solution.py:60
  201.0 8.0 %all-to-all-done = bf16[4,128,1536]{2,1,0:T(8,128)(2,1)S(1)} async-done(((bf16[4,128,1536]{2,1,0:T(8,128)(2,1)}), bf16[4,128,1536]{2,1,0:T(8,128)(2,1)S(1)}, u32[]{:S(2)}, u32[]{:S(2)}) %all-to-all-start) | async-done | bytes 1572896 | tf_op jit(solution)/shard_map/all_to_all | solution.py:16
  209.0 2.3 broadcast_in_dim.13
  211.3 4.3 %all-to-all-start.1 = ((bf16[4,128,1536]{2,1,0:T(8,128)(2,1)}), bf16[4,128,1536]{2,1,0:T(8,128)(2,1)}, u32[]{:S(2)}, u32[]{:S(2)}) async-start(bf16[4,128,1536]{2,1,0:T(8,128)(2,1)} %broadcast_in_dim.13), calls=%async_computation.2 | async-start | bytes 3145728 | tf_op jit(solution)/shard_map/all_to_all | solution.py:16
  215.7 0.3 reduce-scatter.2.cloned.1.call-start
  215.9 6.3 %fusion.13 = bf16[2560,128]{1,0:T(8,128)(2,1)} fusion(f32[2560,128]{1,0:T(8,128)S(1)} %fusion.24, bf16[2560,1536]{1,0:T(8,128)(2,1)} %get-tuple-element.7, bf16[128,1536]{1,0:T(8,128)(2,1)} %param.12), kind=kOutput, calls=%fused_computation.19 | convolution fusion | flops 1007288320 | bytes 10223616 | tf_op jit(solution)/shard_map/dot_general | solution.py:60
  222.2 0.0 reduce-scatter.2.cloned.1.call-update
  222.2 0.7 reduce_sum.89
  222.9 0.2 convert_reduce_fusion.2
  223.1 0.0 copy-start.2
  223.1 0.1 multiply_reduce_fusion.2
  223.3 4.4 %all-gather.3 = f32[2,1,128]{2,1,0:T(1,128)S(1)} all-gather(f32[1,1,128]{2,1,0:T(1,128)S(1)} %bitcast.15), channel_id=3, replica_groups=mesh['rep'=4,'fs'=2,'tp'=16] {'fs'}, dimensions={0}, use_global_device_ids=true | all-gather | bytes 1536 | tf_op jit(solution)/shard_map/all_gather | solution.py:10
  227.7 0.5 reduce_sum.85
  228.2 5.3 %all-to-all-done.1 = bf16[4,128,1536]{2,1,0:T(8,128)(2,1)} async-done(((bf16[4,128,1536]{2,1,0:T(8,128)(2,1)}), bf16[4,128,1536]{2,1,0:T(8,128)(2,1)}, u32[]{:S(2)}, u32[]{:S(2)}) %all-to-all-start.1) | async-done | bytes 1572896 | tf_op jit(solution)/shard_map/all_to_all | solution.py:16
  233.5 1.7 convert_reduce_fusion.1
  235.3 0.0 copy-start.3
  235.3 0.1 multiply_reduce_fusion.1
  235.4 5.3 %all-gather.4 = f32[2,1,128]{2,1,0:T(1,128)S(1)} all-gather(f32[1,1,128]{2,1,0:T(1,128)S(1)} %bitcast.16), channel_id=4, replica_groups=mesh['rep'=4,'fs'=2,'tp'=16] {'fs'}, dimensions={0}, use_global_device_ids=true | all-gather | bytes 1536 | tf_op jit(solution)/shard_map/all_gather | solution.py:10
  240.7 0.5 reduce_sum.87
  241.2 0.0 reduce-scatter.2.cloned.1.call-done
  241.2 0.0 copy-done.2
  241.2 0.0 copy-done.3
Async XLA Ops:
  7.2 188.4 %copy-start = (bf16[128,1536]{1,0:T(8,128)(2,1)S(1)}, bf16[128,1536]{1,0:T(8,128)(2,1)}, u32[]{:S(2)}) copy-start(bf16[128,1536]{1,0:T(8,128)(2,1)} %param.11) | copy-start | bytes 1179652
  7.2 18.8 %all-gather.10.cloned.1.call-start = ((), (), s32[]{:S(2)}) async-start(), calls=%async_computation.7 | async-start | bytes 1966080 | tf_op jit(solution)/shard_map/all_gather | solution.py:31
  9.2 142.2 %all-gather.8.cloned.1.call-start = ((), (), s32[]{:S(2)}) async-start(), calls=%async_computation.5 | async-start | bytes 17825792 | tf_op jit(solution)/shard_map/all_gather | solution.py:45
  41.1 24.4 %all-to-all-start.2 = ((bf16[4,1536,128]{2,1,0:T(8,128)(2,1)}), bf16[4,1536,128]{2,1,0:T(8,128)(2,1)S(1)}, u32[]{:S(2)}, u32[]{:S(2)}) async-start(bf16[4,1536,128]{2,1,0:T(8,128)(2,1)} %broadcast_in_dim.14), calls=%async_computation.3 | async-start | bytes 3145728 | tf_op jit(solution)/shard_map/all_to_all | solution.py:16
  65.7 0.9 copy-start.1
  67.5 118.0 %all-to-all-start.3 = ((f32[16,1,1536]{2,1,0:T(1,128)}), f32[16,1,1536]{2,1,0:T(1,128)S(1)}, u32[]{:S(2)}, u32[]{:S(2)}) async-start(f32[16,1,1536]{2,1,0:T(1,128)} %broadcast_in_dim.15), calls=%async_computation.4 | async-start | bytes 196608 | tf_op jit(solution)/shard_map/all_to_all | solution.py:16
  186.8 22.2 %all-to-all-start = ((bf16[4,128,1536]{2,1,0:T(8,128)(2,1)}), bf16[4,128,1536]{2,1,0:T(8,128)(2,1)S(1)}, u32[]{:S(2)}, u32[]{:S(2)}) async-start(bf16[4,128,1536]{2,1,0:T(8,128)(2,1)} %broadcast_in_dim.12), calls=%async_computation.1 | async-start | bytes 3145728 | tf_op jit(solution)/shard_map/all_to_all | solution.py:16
  211.3 22.2 %all-to-all-start.1 = ((bf16[4,128,1536]{2,1,0:T(8,128)(2,1)}), bf16[4,128,1536]{2,1,0:T(8,128)(2,1)}, u32[]{:S(2)}, u32[]{:S(2)}) async-start(bf16[4,128,1536]{2,1,0:T(8,128)(2,1)} %broadcast_in_dim.13), calls=%async_computation.2 | async-start | bytes 3145728 | tf_op jit(solution)/shard_map/all_to_all | solution.py:16
  215.7 25.6 %reduce-scatter.2.cloned.1.call-start = ((), (), s32[]{:S(2)}) async-start(), calls=%async_computation.6 | async-start | bytes 983040 | tf_op jit(solution)/shard_map/reduce_scatter | solution.py:87
  223.1 18.1 %copy-start.2 = (f32[128,1536]{1,0:T(8,128)}, f32[128,1536]{1,0:T(8,128)S(1)}, u32[]{:S(2)}) copy-start(f32[128,1536]{1,0:T(8,128)S(1)} %convert_reduce_fusion.2) | copy-start | bytes 2359300
  235.3 6.0 %copy-start.3 = (f32[128,1536]{1,0:T(8,128)}, f32[128,1536]{1,0:T(8,128)S(1)}, u32[]{:S(2)}) copy-start(f32[128,1536]{1,0:T(8,128)S(1)} %convert_reduce_fusion.1) | copy-start | bytes 2359300
Sparse Core Ops, SparseCore 0:
  10.2 15.7 all-gather.9
  31.3 120.1 all-gather.7
  222.3 12.9 reduce-scatter.1
where the time goes:
time: 248 us
  waiting for transfers between devices  127 us (51%)
  matrix products  59.5 us (24%)
  starting transfers between devices  19 us (8%)
  between operations  13.9 us (6%)
  local copies, waits for them, and re-layouts  10.1 us (4%)
  blocking collectives  9.71 us (4%)
  other arithmetic  8.46 us (3%)
    all_gather x1, waiting for transfers between devices, sent_together(): lax.all_gather(both, axis, axis=dim, tiled=True)  77.2 us
    dot_general x3, matrix products, contract_cols(): lax.dot_general(left_side, right_side, (((1,), (1,)), ((), ())), preferre...  41.3 us
    all_to_all x4, waiting for transfers between devices, copy_for_each(): return lax.all_to_all(copies, axis, split_axis=0, concat_axis=0, tiled=True)  33.1 us
    all_to_all x4, starting transfers between devices, copy_for_each(): return lax.all_to_all(copies, axis, split_axis=0, concat_axis=0, tiled=True)  18.7 us
    dot_general x3, matrix products, contract_rows(): lax.dot_general(left_side, right_side, (((0,), (0,)), ((), ())), preferre...  18.2 us
    all_gather x1, waiting for transfers between devices, gather_packed(): lines, at, gathered = (lax.all_gather(ravelled, axis), 0, [])  16.7 us
    all_gather x2, blocking collectives, gathered_total(): tiles = lax.all_gather(x, axis)  9.71 us
    broadcast_in_dim x4, local copies, waits for them, and re-layouts, copy_for_each(): copies = jnp.broadcast_to(x, (lax.axis_size(axis), *x.shape))  5.59 us
  transfers between devices with their start and end apart: 7, of which 5 were waited for; matrix products, arithmetic and copies ran while one was open for 27% of the time, Pallas kernels for 0%

commit v1 on v0

v1 whole, which is shorter than its diff:
```python
import math

import jax
import jax.numpy as jnp
from jax import lax
from jax.experimental import pallas as pl
from jax.experimental.pallas import tpu as pltpu
from jax.sharding import PartitionSpec as P

MESH = pl.DeviceIdType.MESH
BF = jnp.bfloat16
F32 = jnp.float32

TOK = 2560
HALF = 1280
FH = 1536
N = 256
CH = 256
NCH = FH // CH
NCOT = HALF // N
NPAY = NCOT + NCH
TM = 640
TP = 256


def body(
    x_hbm, cot_hbm, gate_hbm, up_hbm, gw_hbm, uw_hbm, dw_hbm,
    ig_out, gg_out, ug_out, dg_out, gsq_out, usq_out, dsq_out,
    allb, aa, cc, gbuf, ubuf, hid, xb, xt, dgt, ig, gw, uw,
    gacc, gs, rs, ag, ds, dr, dag, igs, igr, sqacc, sqs, sqr, dsqs, dsqr,
    send_sem, recv_sem, d2d_send, d2d_recv, loc_sem, tile_sem,
    rs_send, rs_recv, ag_send, ag_recv, q_send, q_recv, r_send, r_recv,
):
    rep = lax.axis_index("rep")
    fs = lax.axis_index("fs")
    tp = lax.axis_index("tp")
    z, y = tp // 4, tp % 4
    sib = 1 - fs
    scale = 1.0 / math.sqrt(TOK * 4)

    def blk(dz, dy):
        return ((z + dz) % 4) * 4 + (y + dy) % 4

    mine = pl.multiple_of(fs * HALF, HALF)
    theirs = pl.multiple_of(sib * HALF, HALF)

    own_cot = pltpu.make_async_copy(cot_hbm, allb.at[tp, pl.ds(mine, HALF)], loc_sem.at[0])
    own_dw = pltpu.make_async_copy(dw_hbm, allb.at[tp, pl.ds(TOK, FH)], loc_sem.at[1])
    own_x = pltpu.make_async_copy(x_hbm, xb.at[pl.ds(mine, HALF)], loc_sem.at[2])
    own_gw = pltpu.make_async_copy(gw_hbm, gw, loc_sem.at[3])
    own_uw = pltpu.make_async_copy(uw_hbm, uw, loc_sem.at[4])
    own_cot.start()
    own_x.start()
    own_dw.start()

    def tile_rows(i):
        return pl.multiple_of(((fs * 5 + i) % 10) * TP, TP)

    def loads(i):
        slot = i % 2
        r = tile_rows(i)
        return (
            pltpu.make_async_copy(gate_hbm.at[pl.ds(r, TP)], gbuf.at[slot], tile_sem.at[slot, 0]),
            pltpu.make_async_copy(up_hbm.at[pl.ds(r, TP)], ubuf.at[slot], tile_sem.at[slot, 1]),
        )

    for c in loads(0):
        c.start()
    for c in loads(1):
        c.start()
    own_gw.start()
    own_uw.start()

    barrier = pltpu.get_barrier_semaphore()
    for d in range(1, 16):
        pl.semaphore_signal(barrier, inc=1, device_id={"tp": (tp + d) % 16}, device_id_type=MESH)
    for d in range(1, 4):
        pl.semaphore_signal(barrier, inc=1, device_id={"rep": (rep + d) % 4}, device_id_type=MESH)
    pl.semaphore_signal(barrier, inc=1, device_id={"fs": sib}, device_id_type=MESH)
    pl.semaphore_wait(barrier, 19)

    def row0(p):
        w = (p + 11) // 16
        return 256 * p + HALF * (w + fs * (1 - w))

    def put(p, b, off, n, dz, dy, g):
        rows = pl.ds(pl.multiple_of(row0(p) + off, 64), n)
        ref = allb.at[b, rows]
        pltpu.make_async_remote_copy(
            src_ref=ref,
            dst_ref=ref,
            send_sem=send_sem.at[p],
            recv_sem=recv_sem.at[p, g],
            device_id={"tp": blk(dz, dy)},
            device_id_type=MESH,
        ).start()

    def take(sem, k):
        ref = allb.at[pl.ds(0, k), pl.ds(0, N)]
        pltpu.make_async_copy(ref, ref, sem).wait()

    H, Q = N // 2, N // 4
    OA, OB = 0, H

    def both_y(p, b, g):
        put(p, b, OA, H, 0, 1, g)
        put(p, b, OA, H, 0, -1, g)

    def both_z(p, b, g):
        put(p, b, OB, H, 1, 0, g)
        put(p, b, OB, H, -1, 0, g)

    def r0(p):
        put(p, tp, OA, H, 1, 0, 0)
        put(p, tp, OA, H, -1, 0, 0)
        put(p, tp, OB, H, 0, 1, 0)
        put(p, tp, OB, H, 0, -1, 0)
        both_y(p, tp, 2)
        both_z(p, tp, 2)

    def r1(p):
        take(recv_sem.at[p, 0], 2)
        put(p, blk(-1, 0), OA, Q, 1, 0, 1)
        put(p, blk(1, 0), OA + Q, Q, -1, 0, 1)
        put(p, blk(0, -1), OB, Q, 0, 1, 1)
        put(p, blk(0, 1), OB + Q, Q, 0, -1, 1)
        for d in (-1, 1):
            both_y(p, blk(d, 0), 2)
            both_z(p, blk(0, d), 2)

    def r2(p):
        take(recv_sem.at[p, 1], 1)
        both_y(p, blk(2, 0), 3)
        both_z(p, blk(0, 2), 3)

    def onward(p, d, g):
        put(p, blk(d, -1), OA, Q, 0, 1, g)
        put(p, blk(d, 1), OA + Q, Q, 0, -1, g)
        put(p, blk(-1, d), OB, Q, 1, 0, g)
        put(p, blk(1, d), OB + Q, Q, -1, 0, g)

    def r3(p):
        take(recv_sem.at[p, 2], 6)
        for d in (0, -1, 1):
            onward(p, d, 4)

    def r4(p):
        take(recv_sem.at[p, 3], 2)
        onward(p, 2, 5)

    def r5(p):
        take(recv_sem.at[p, 4], 3)
        take(recv_sem.at[p, 5], 1)

    def to_sibling(p):
        rows = pl.ds(pl.multiple_of(fs * HALF + N * p, N), N)
        for d in range(1, 16):
            ref = allb.at[(tp + d) % 16, rows]
            pltpu.make_async_remote_copy(
                src_ref=ref,
                dst_ref=ref,
                send_sem=d2d_send.at[p],
                recv_sem=d2d_recv.at[p],
                device_id={"fs": sib},
                device_id_type=MESH,
            ).start()

    def d2d(src, dst, k):
        return pltpu.make_async_remote_copy(
            src_ref=src,
            dst_ref=dst,
            send_sem=r_send.at[k],
            recv_sem=r_recv.at[k],
            device_id={"fs": sib},
            device_id_type=MESH,
        )

    own_cot.wait()
    r0(0)
    cot_pair = d2d(allb.at[tp, pl.ds(mine, HALF)], allb.at[tp, pl.ds(mine, HALF)], 0)
    cot_pair.start()
    own_x.wait()
    x_pair = d2d(xb.at[pl.ds(mine, HALF)], xb.at[pl.ds(mine, HALF)], 1)
    x_pair.start()
    own_dw.wait()
    own_gw.wait()
    own_uw.wait()
    dgt[...] = jnp.zeros_like(dgt)
    ig[...] = jnp.zeros_like(ig)
    sqacc[...] = jnp.zeros_like(sqacc)
    cot_pair.wait_recv()
    x_pair.wait_recv()
    r1(0)

    def transpose_x(i, carry):
        r = pl.multiple_of(i * 128, 128)
        v = xb[pl.ds(r, 128), :].astype(F32)
        xt[i // 5, :, pl.ds(pl.multiple_of((i % 5) * 128, 128), 128)] = v.T.astype(BF)
        return carry

    lax.fori_loop(0, TOK // 128, transpose_x, 0)

    def tile(i):
        slot = i % 2
        r = tile_rows(i)
        for c in loads(i):
            c.wait()

        def sub(k, carry):
            q = pl.multiple_of(k * 32, 32)
            for j in range(NCH):
                g = gbuf[slot, pl.ds(q, 32), j * CH : (j + 1) * CH].astype(F32)
                u = ubuf[slot, pl.ds(q, 32), j * CH : (j + 1) * CH].astype(F32)
                s = 1.0 / (1.0 + jnp.exp(-g))
                a = g * s
                hid[pl.ds(q, 32), j * CH : (j + 1) * CH] = (a * u).astype(BF)
                aa[j, pl.ds(pl.multiple_of(r + q, 32), 32), :] = a.astype(BF)
                cc[j, pl.ds(pl.multiple_of(r + q, 32), 32), :] = (
                    u * s * (1.0 + g * (1.0 - s))
                ).astype(BF)
            return carry

        lax.fori_loop(0, TP // 32, sub, 0)

        @pl.when(i < 8)
        def _():
            for c in loads(i + 2):
                c.start()

        ct = allb[tp, pl.ds(r, TP), :].astype(F32).T.astype(BF)
        dgt[...] += jnp.dot(ct, hid[...], preferred_element_type=F32)

    def first(p, carry):
        r2(p)
        r0(p + 1)

        @pl.when(p >= 1)
        def _():
            r5(p - 1)
            to_sibling(p - 1)

        tile(2 * p)
        r3(p)
        r1(p + 1)
        tile(2 * p + 1)
        r4(p)
        return carry

    lax.fori_loop(0, NCOT, first, 0)

    def scatter(src, dst, s_sem, r_sem):
        for d in range(1, 4):
            peer = (rep + d) % 4
            pltpu.make_async_remote_copy(
                src_ref=src.at[peer],
                dst_ref=dst.at[rep],
                send_sem=s_sem,
                recv_sem=r_sem,
                device_id={"rep": peer},
                device_id_type=MESH,
            ).start()

    def spread(buf, s_sem, r_sem):
        for d in range(1, 4):
            pltpu.make_async_remote_copy(
                src_ref=buf.at[rep],
                dst_ref=buf.at[rep],
                send_sem=s_sem,
                recv_sem=r_sem,
                device_id={"rep": (rep + d) % 4},
                device_id_type=MESH,
            ).start()

    def three(buf, sem):
        ref = buf.at[pl.ds(0, 3)]
        pltpu.make_async_copy(ref, ref, sem).wait()

    p = NCOT
    r2(p)
    r0(p + 1)
    r5(p - 1)
    to_sibling(p - 1)
    for j in range(4):
        ds[j] = (dgt[32 * j : 32 * j + 32, :] * scale).astype(BF)
    dr[rep] = ds[rep]
    r3(p)
    scatter(ds, dr, rs_send.at[NCH], rs_recv.at[NCH])
    r1(p + 1)
    r4(p)
    for k in range(NCOT):
        take(d2d_recv.at[k], 15)

    def main_tile(c, j):
        t = (sib * 2 + j) % 4
        rows = pl.ds(pl.multiple_of(t * TM, TM), TM)
        fr = pl.ds(pl.multiple_of(TOK + c * CH, CH), CH)
        lhs = jnp.concatenate([allb[k, rows, :] for k in range(16)], axis=1)
        rhs = jnp.concatenate([allb[k, fr, :] for k in range(16)], axis=1)
        hg = lax.dot_general(lhs, rhs, (((1,), (1,)), ((), ())), preferred_element_type=F32)
        gd = (hg * cc[c, rows, :].astype(F32)).astype(BF)
        ud = (hg * aa[c, rows, :].astype(F32)).astype(BF)
        cols = pl.ds(pl.multiple_of(c * CH, CH), CH)
        both = jnp.concatenate([gd, ud], axis=1)
        wts = jnp.concatenate([gw[:, cols], uw[:, cols]], axis=1)
        ig[rows, :] += lax.dot_general(
            both, wts, (((1,), (1,)), ((), ())), preferred_element_type=F32
        )
        gu = jnp.dot(xt[t], both, preferred_element_type=F32)
        if j == 0:
            gacc[...] = gu
        else:
            gacc[...] += gu

    def send_grads(c):
        for j in range(4):
            gs[c, j, 0:32, :] = (gacc[32 * j : 32 * j + 32, 0:CH] * scale).astype(BF)
            gs[c, j, 32:64, :] = (gacc[32 * j : 32 * j + 32, CH : 2 * CH] * scale).astype(BF)
        rs[c, rep] = gs[c, rep]
        scatter(gs.at[c], rs.at[c], rs_send.at[c], rs_recv.at[c])

    def reduce_grads(c):
        three(rs.at[c], rs_recv.at[c])
        v = rs[c, 0].astype(F32) + rs[c, 1].astype(F32)
        v = v + rs[c, 2].astype(F32) + rs[c, 3].astype(F32)
        ag[c, rep] = v.astype(BF)
        spread(ag.at[c], ag_send.at[c], ag_recv.at[c])

    def finish_grads(c):
        three(ag.at[c], ag_recv.at[c])
        cols = pl.ds(pl.multiple_of(c * CH, CH), CH)
        for j in range(4):
            v = ag[c, j].astype(F32)
            gg_out[32 * j : 32 * j + 32, cols] = v[0:32]
            ug_out[32 * j : 32 * j + 32, cols] = v[32:64]
            w = v * v
            w = w[:, 0:128] + w[:, 128:256]
            sqacc[32 * j : 32 * j + 32, :] += w[0:32]
            sqacc[128 + 32 * j : 160 + 32 * j, :] += w[32:64]

    def reduce_down():
        three(dr, rs_recv.at[NCH])
        v = dr[0].astype(F32) + dr[1].astype(F32)
        v = v + dr[2].astype(F32) + dr[3].astype(F32)
        dag[rep] = v.astype(BF)
        spread(dag, ag_send.at[NCH], ag_recv.at[NCH])

    def finish_down():
        three(dag, ag_recv.at[NCH])
        for k in range(FH // 128):
            v = jnp.concatenate(
                [dag[j, :, 128 * k : 128 * k + 128].astype(F32) for j in range(4)], axis=0
            )
            dg_out[128 * k : 128 * k + 128, :] = v.T
            dsqs[:, 128 * k : 128 * k + 128] = jnp.sum(v * v, axis=0, keepdims=True)

    def send_down_sq():
        dsqr[tp] = dsqs[...]
        for d in range(1, 16):
            pltpu.make_async_remote_copy(
                src_ref=dsqs,
                dst_ref=dsqr.at[tp],
                send_sem=q_send,
                recv_sem=q_recv,
                device_id={"tp": (tp + d) % 16},
                device_id_type=MESH,
            ).start()

    ig_pair = d2d(igs, igr, 2)

    def chunk(c, carry):
        p = NCOT + 1 + c

        @pl.when(p < NPAY)
        def _():
            r2(p)

        @pl.when(p + 1 < NPAY)
        def _():
            r0(p + 1)

        r5(p - 1)
        main_tile(c, 0)

        @pl.when(p < NPAY)
        def _():
            r3(p)

        @pl.when(c == 0)
        def _():
            reduce_down()

        main_tile(c, 1)

        @pl.when(p + 1 < NPAY)
        def _():
            r1(p + 1)

        @pl.when(c >= 1)
        def _():
            reduce_grads(c - 1)

        @pl.when(c == NCH - 1)
        def _():
            igs[...] = ig[pl.ds(theirs, HALF), :].astype(BF)

        main_tile(c, 2)

        @pl.when(c == NCH - 1)
        def _():
            ig_pair.start()

        @pl.when(p < NPAY)
        def _():
            r4(p)

        @pl.when(c >= 2)
        def _():
            finish_grads(c - 2)

        @pl.when(c == 1)
        def _():
            finish_down()

        main_tile(c, 3)

        @pl.when(c == 1)
        def _():
            send_down_sq()

        send_grads(c)
        return carry

    lax.fori_loop(0, NCH, chunk, 0)

    finish_grads(NCH - 2)
    ig_pair.wait_recv()
    mine_part = ig[pl.ds(mine, HALF), :].astype(BF).astype(F32)
    ig_out[...] = (mine_part + igr[...].astype(F32)).astype(BF)
    reduce_grads(NCH - 1)
    all15 = dsqr.at[pl.ds(0, 15)]
    pltpu.make_async_copy(all15, all15, q_recv).wait()
    total = dsqr[0]
    for k in range(1, 16):
        total = total + dsqr[k]
    dsq_out[...] = total
    finish_grads(NCH - 1)
    sqs[...] = jnp.sum(sqacc[...].T, axis=0, keepdims=True)
    sq_pair = d2d(sqs, sqr, 3)
    sq_pair.start()

    for p in range(NPAY):
        take(send_sem.at[p], 15)
    for k in range(NCOT):
        take(d2d_send.at[k], 15)
    for k in range(NCH):
        three(gs.at[k], rs_send.at[k])
        three(ag.at[k], ag_send.at[k])
    three(ds, rs_send.at[NCH])
    three(dag, ag_send.at[NCH])
    pltpu.make_async_copy(all15, all15, q_send).wait()
    cot_pair.wait_send()
    x_pair.wait_send()
    ig_pair.wait_send()
    sq_pair.wait()
    both_sq = sqs[...] + sqr[...]
    gsq_out[...] = both_sq[:, 0:128]
    usq_out[...] = both_sq[:, 128:256]


def on_device(layer_input, cotangent, gate_pre, up_pre, gate_weight, up_weight, down_weight):
    anyspec = pl.BlockSpec(memory_space=pl.ANY)
    vm = pl.BlockSpec(memory_space=pltpu.VMEM)
    dma = pltpu.SemaphoreType.DMA
    outs = pl.pallas_call(
        body,
        out_shape=(
            jax.ShapeDtypeStruct((HALF, 128), BF),
            jax.ShapeDtypeStruct((128, FH), F32),
            jax.ShapeDtypeStruct((128, FH), F32),
            jax.ShapeDtypeStruct((FH, 128), F32),
            jax.ShapeDtypeStruct((1, 128), F32),
            jax.ShapeDtypeStruct((1, 128), F32),
            jax.ShapeDtypeStruct((1, FH), F32),
        ),
        in_specs=[anyspec] * 7,
        out_specs=(vm,) * 7,
        scratch_shapes=[
            pltpu.VMEM((16, TOK + FH, 128), BF),
            pltpu.VMEM((NCH, TOK, CH), BF),
            pltpu.VMEM((NCH, TOK, CH), BF),
            pltpu.VMEM((2, TP, FH), BF),
            pltpu.VMEM((2, TP, FH), BF),
            pltpu.VMEM((TP, FH), BF),
            pltpu.VMEM((TOK, 128), BF),
            pltpu.VMEM((4, 128, TM), BF),
            pltpu.VMEM((128, FH), F32),
            pltpu.VMEM((TOK, 128), F32),
            pltpu.VMEM((128, FH), BF),
            pltpu.VMEM((128, FH), BF),
            pltpu.VMEM((128, 2 * CH), F32),
            pltpu.VMEM((NCH, 4, 64, CH), BF),
            pltpu.VMEM((NCH, 4, 64, CH), BF),
            pltpu.VMEM((NCH, 4, 64, CH), BF),
            pltpu.VMEM((4, 32, FH), BF),
            pltpu.VMEM((4, 32, FH), BF),
            pltpu.VMEM((4, 32, FH), BF),
            pltpu.VMEM((HALF, 128), BF),
            pltpu.VMEM((HALF, 128), BF),
            pltpu.VMEM((256, 128), F32),
            pltpu.VMEM((1, 256), F32),
            pltpu.VMEM((1, 256), F32),
            pltpu.VMEM((1, FH), F32),
            pltpu.VMEM((16, 1, FH), F32),
            dma((NPAY,)),
            dma((NPAY, 6)),
            dma((NCOT,)),
            dma((NCOT,)),
            dma((5,)),
            dma((2, 2)),
            dma((NCH + 1,)),
            dma((NCH + 1,)),
            dma((NCH + 1,)),
            dma((NCH + 1,)),
            dma,
            dma,
            dma((4,)),
            dma((4,)),
        ],
        compiler_params=pltpu.CompilerParams(
            collective_id=0, has_side_effects=True, vmem_limit_bytes=64000000
        ),
        name="backward",
    )(layer_input, cotangent, gate_pre, up_pre, gate_weight, up_weight, down_weight)
    ig, gg, ug, dg, gsq, usq, dsq = outs
    return ig, gg, ug, dg, gsq.reshape(128), usq.reshape(128), dsq.reshape(FH)


def solution(mesh):
    return jax.shard_map(
        on_device,
        mesh=mesh,
        in_specs=(
            P(("rep", "fs"), "tp"),
            P(("rep", "fs"), "tp"),
            P("rep", "fs"),
            P("rep", "fs"),
            P("tp", "fs"),
            P("tp", "fs"),
            P("fs", "tp"),
        ),
        out_specs=(
            P(("rep", "fs"), "tp"),
            P("tp", "fs"),
            P("tp", "fs"),
            P("fs", "tp"),
            P("tp"),
            P("tp"),
            P("fs"),
        ),
        check_vma=False,
    )
```

time: 248 us -> 140 us (0.56)
  Pallas kernels: 0 us -> 127 us
  waiting for transfers between devices: 127 us -> 0 us
  matrix products: 59.5 us -> 0 us
  starting transfers between devices: 19 us -> 0 us
  between operations: 13.9 us -> 0.65 us
  blocking collectives: 9.71 us -> 0 us
  other arithmetic: 8.46 us -> 1.31 us
    pallas_call x0 -> x1, Pallas kernels: none -> 127 us  [on_device(): pl.pallas_call(body, out_shape=(jax.ShapeDtypeStruct((HALF, 128), BF), ja...]
    all_gather x2 -> x0, waiting for transfers between devices: 93.9 us -> none  [the longest x1 77.2 us: sent_together(): lax.all_gather(both, axis, axis=dim, tiled=True)]
    dot_general x6 -> x0, matrix products: 59.5 us -> none  [the longest x3 41.3 us: contract_cols(): lax.dot_general(left_side, right_side, (((1,), (1,)), ((), ())), preferre...]
    all_to_all x4 -> x0, waiting for transfers between devices: 33.1 us -> none  [copy_for_each(): return lax.all_to_all(copies, axis, split_axis=0, concat_axis=0, tiled=True)]
    all_to_all x4 -> x0, starting transfers between devices: 18.7 us -> none  [copy_for_each(): return lax.all_to_all(copies, axis, split_axis=0, concat_axis=0, tiled=True)]
    all_gather x2 -> x0, blocking collectives: 9.71 us -> none  [gathered_total(): tiles = lax.all_gather(x, axis)]
    unnamed x8 -> x6, local copies, waits for them, and re-layouts: 0.9 us -> 10.3 us
    broadcast_in_dim x4 -> x0, local copies, waits for them, and re-layouts: 5.59 us -> none  [copy_for_each(): copies = jnp.broadcast_to(x, (lax.axis_size(axis), *x.shape))]
  transfers between devices with their start and end apart: 7 -> 0, of which waited for: 5 -> 0; matrix products, arithmetic and copies ran while one was open for 27% -> 0% of each run, Pallas kernels for 0% -> 0%
where the time goes in v1:
time: 140 us; the launch traced here: 139 us
  Pallas kernels  127 us (91%)
  local copies, waits for them, and re-layouts  10.3 us (7%)
    pallas_call x1, Pallas kernels, on_device(): pl.pallas_call(body, out_shape=(jax.ShapeDtypeStruct((HALF, 128), BF), ja...  127 us
    unnamed x6, local copies, waits for them, and re-layouts  10.3 us

profile of v1, /device:TPU:1, one launch (start us, length us, event | category | flops | bytes accessed | tf_op | source)
XLA Modules:
  0.0 139.3 jit_solution(1268360534335931845)
XLA Ops:
  0.6 127.1 %backward.1 = (bf16[1280,128]{1,0:T(8,128)(2,1)}, f32[128,1536]{1,0:T(8,128)}, f32[128,1536]{1,0:T(8,128)}, f32[1536,128]{1,0:T(8,128)}, f32[1,128]{1,0:T(1,128)}, /*index=5*/f32[1,128]{1,0:T(1,128)}, f32[1,1536]{1,0:T(1,128)}) custom-call(bf16[1280,128]{1,0:T(8,128)(2,1)} %x_hbm.1, bf16[1280,128]{1,0:T(8,128)(2,1)} %cot_hbm.1, bf16[2560,1536]{1,0:T(8,128)(2,1)} %gate_hbm.1, ...), custom_call_target="tpu_custom_call" | custom-call | tf_op jit(solution)/shard_map/backward/pallas_call | solution.py:474
  127.7 1.3 reduce
  129.0 1.7 %copy.20 = bf16[1280,128]{1,0:T(8,128)(2,1)} copy(bf16[1280,128]{1,0:T(8,128)(2,1)} %get-tuple-element.28) | data formatting | bytes 655360
  130.8 2.1 %copy.21 = f32[128,1536]{1,0:T(8,128)} copy(f32[128,1536]{1,0:T(8,128)} %get-tuple-element.29) | data formatting | bytes 1572864
  132.8 2.1 %copy.22 = f32[128,1536]{1,0:T(8,128)} copy(f32[128,1536]{1,0:T(8,128)} %get-tuple-element.30) | data formatting | bytes 1572864
  134.9 2.1 %copy.23 = f32[1536,128]{1,0:T(8,128)} copy(f32[1536,128]{1,0:T(8,128)} %get-tuple-element.31) | data formatting | bytes 1572864
  137.0 1.2 copy.24
  138.1 1.2 copy.25

commit v2 on v1

--- a/solution.py
+++ b/solution.py
@@ -25,9 +25,9 @@
 
 def body(
     x_hbm, cot_hbm, gate_hbm, up_hbm, gw_hbm, uw_hbm, dw_hbm,
-    ig_out, gg_out, ug_out, dg_out, gsq_out, usq_out, dsq_out,
+    ig_out, ag, dag, sq_out, dsq_out,
     allb, aa, cc, gbuf, ubuf, hid, xb, xt, dgt, ig, gw, uw,
-    gacc, gs, rs, ag, ds, dr, dag, igs, igr, sqacc, sqs, sqr, dsqs, dsqr,
+    gb, gacc, gs, rs, ds, dr, igs, igr, sqacc, sqs, sqr, dsqs, dsqr,
     send_sem, recv_sem, d2d_send, d2d_recv, loc_sem, tile_sem,
     rs_send, rs_recv, ag_send, ag_recv, q_send, q_recv, r_send, r_recv,
 ):
@@ -75,9 +75,11 @@
     for d in range(1, 16):
         pl.semaphore_signal(barrier, inc=1, device_id={"tp": (tp + d) % 16}, device_id_type=MESH)
     for d in range(1, 4):
-        pl.semaphore_signal(barrier, inc=1, device_id={"rep": (rep + d) % 4}, device_id_type=MESH)
+        peer = (rep + d) % 4
+        pl.semaphore_signal(barrier, inc=1, device_id={"rep": peer}, device_id_type=MESH)
+        pl.semaphore_signal(barrier, inc=1, device_id={"rep": peer, "fs": sib}, device_id_type=MESH)
     pl.semaphore_signal(barrier, inc=1, device_id={"fs": sib}, device_id_type=MESH)
-    pl.semaphore_wait(barrier, 19)
+    pl.semaphore_wait(barrier, 22)
 
     def row0(p):
         w = (p + 11) // 16
@@ -177,6 +179,7 @@
 
     own_cot.wait()
     r0(0)
+    r0(1)
     cot_pair = d2d(allb.at[tp, pl.ds(mine, HALF)], allb.at[tp, pl.ds(mine, HALF)], 0)
     cot_pair.start()
     own_x.wait()
@@ -188,14 +191,14 @@
     dgt[...] = jnp.zeros_like(dgt)
     ig[...] = jnp.zeros_like(ig)
     sqacc[...] = jnp.zeros_like(sqacc)
+    r1(0)
     cot_pair.wait_recv()
     x_pair.wait_recv()
-    r1(0)
 
     def transpose_x(i, carry):
         r = pl.multiple_of(i * 128, 128)
         v = xb[pl.ds(r, 128), :].astype(F32)
-        xt[i // 5, :, pl.ds(pl.multiple_of((i % 5) * 128, 128), 128)] = v.T.astype(BF)
+        xt[:, pl.ds(r, 128)] = v.T.astype(BF)
         return carry
 
     lax.fori_loop(0, TOK // 128, transpose_x, 0)
@@ -230,20 +233,24 @@
         ct = allb[tp, pl.ds(r, TP), :].astype(F32).T.astype(BF)
         dgt[...] += jnp.dot(ct, hid[...], preferred_element_type=F32)
 
-    def first(p, carry):
-        r2(p)
-        r0(p + 1)
-
-        @pl.when(p >= 1)
-        def _():
-            r5(p - 1)
-            to_sibling(p - 1)
-
-        tile(2 * p)
-        r3(p)
-        r1(p + 1)
-        tile(2 * p + 1)
-        r4(p)
+    def first(k, carry):
+        r2(k)
+        r1(k + 1)
+        tile(2 * k)
+        r3(k)
+
+        @pl.when(k >= 1)
+        def _():
+            r4(k - 1)
+
+        r0(k + 2)
+        tile(2 * k + 1)
+
+        @pl.when(k >= 2)
+        def _():
+            r5(k - 2)
+            to_sibling(k - 2)
+
         return carry
 
     lax.fori_loop(0, NCOT, first, 0)
@@ -275,41 +282,43 @@
         ref = buf.at[pl.ds(0, 3)]
         pltpu.make_async_copy(ref, ref, sem).wait()
 
-    p = NCOT
-    r2(p)
-    r0(p + 1)
-    r5(p - 1)
-    to_sibling(p - 1)
-    for j in range(4):
-        ds[j] = (dgt[32 * j : 32 * j + 32, :] * scale).astype(BF)
-    dr[rep] = ds[rep]
-    r3(p)
-    scatter(ds, dr, rs_send.at[NCH], rs_recv.at[NCH])
-    r1(p + 1)
-    r4(p)
+    for k in range(NCOT, NCOT + 2):
+        r2(k)
+        r1(k + 1)
+        if k == NCOT:
+            for j in range(4):
+                ds[j] = (dgt[32 * j : 32 * j + 32, :] * scale).astype(BF)
+            dr[rep] = ds[rep]
+        r3(k)
+        if k == NCOT:
+            scatter(ds, dr, rs_send.at[NCH], rs_recv.at[NCH])
+        r4(k - 1)
+        r0(k + 2)
+        r5(k - 2)
+        to_sibling(k - 2)
     for k in range(NCOT):
         take(d2d_recv.at[k], 15)
 
     def main_tile(c, j):
-        t = (sib * 2 + j) % 4
-        rows = pl.ds(pl.multiple_of(t * TM, TM), TM)
+        rows = pl.ds(j * TM, TM)
         fr = pl.ds(pl.multiple_of(TOK + c * CH, CH), CH)
         lhs = jnp.concatenate([allb[k, rows, :] for k in range(16)], axis=1)
         rhs = jnp.concatenate([allb[k, fr, :] for k in range(16)], axis=1)
         hg = lax.dot_general(lhs, rhs, (((1,), (1,)), ((), ())), preferred_element_type=F32)
         gd = (hg * cc[c, rows, :].astype(F32)).astype(BF)
         ud = (hg * aa[c, rows, :].astype(F32)).astype(BF)
+        gb[rows, 0:CH] = gd
+        gb[rows, CH : 2 * CH] = ud
+
+    def main_grads():
+        gacc[...] = jnp.dot(xt[...], gb[...], preferred_element_type=F32)
+
+    def main_input(c):
         cols = pl.ds(pl.multiple_of(c * CH, CH), CH)
-        both = jnp.concatenate([gd, ud], axis=1)
         wts = jnp.concatenate([gw[:, cols], uw[:, cols]], axis=1)
-        ig[rows, :] += lax.dot_general(
-            both, wts, (((1,), (1,)), ((), ())), preferred_element_type=F32
+        ig[...] += lax.dot_general(
+            gb[...], wts, (((1,), (1,)), ((), ())), preferred_element_type=F32
         )
-        gu = jnp.dot(xt[t], both, preferred_element_type=F32)
-        if j == 0:
-            gacc[...] = gu
-        else:
-            gacc[...] += gu
 
     def send_grads(c):
         for j in range(4):
@@ -324,18 +333,10 @@
         v = v + rs[c, 2].astype(F32) + rs[c, 3].astype(F32)
         ag[c, rep] = v.astype(BF)
         spread(ag.at[c], ag_send.at[c], ag_recv.at[c])
-
-    def finish_grads(c):
-        three(ag.at[c], ag_recv.at[c])
-        cols = pl.ds(pl.multiple_of(c * CH, CH), CH)
-        for j in range(4):
-            v = ag[c, j].astype(F32)
-            gg_out[32 * j : 32 * j + 32, cols] = v[0:32]
-            ug_out[32 * j : 32 * j + 32, cols] = v[32:64]
-            w = v * v
-            w = w[:, 0:128] + w[:, 128:256]
-            sqacc[32 * j : 32 * j + 32, :] += w[0:32]
-            sqacc[128 + 32 * j : 160 + 32 * j, :] += w[32:64]
+        w = v * v
+        w = w[:, 0:128] + w[:, 128:256]
+        sqacc[pl.ds(pl.multiple_of(32 * rep, 32), 32), :] += w[0:32]
+        sqacc[pl.ds(pl.multiple_of(128 + 32 * rep, 32), 32), :] += w[32:64]
 
     def reduce_down():
         three(dr, rs_recv.at[NCH])
@@ -350,7 +351,6 @@
             v = jnp.concatenate(
                 [dag[j, :, 128 * k : 128 * k + 128].astype(F32) for j in range(4)], axis=0
             )
-            dg_out[128 * k : 128 * k + 128, :] = v.T
             dsqs[:, 128 * k : 128 * k + 128] = jnp.sum(v * v, axis=0, keepdims=True)
 
     def send_down_sq():
@@ -368,22 +368,22 @@
     ig_pair = d2d(igs, igr, 2)
 
     def chunk(c, carry):
-        p = NCOT + 1 + c
-
-        @pl.when(p < NPAY)
-        def _():
-            r2(p)
-
-        @pl.when(p + 1 < NPAY)
-        def _():
-            r0(p + 1)
-
-        r5(p - 1)
+        k = NCOT + 2 + c
+
+        @pl.when(k < NPAY)
+        def _():
+            r2(k)
+
+        @pl.when(k + 1 < NPAY)
+        def _():
+            r1(k + 1)
+
+        r5(k - 2)
         main_tile(c, 0)
 
-        @pl.when(p < NPAY)
-        def _():
-            r3(p)
+        @pl.when(k < NPAY)
+        def _():
+            r3(k)
 
         @pl.when(c == 0)
         def _():
@@ -391,31 +391,19 @@
 
         main_tile(c, 1)
 
-        @pl.when(p + 1 < NPAY)
-        def _():
-            r1(p + 1)
+        @pl.when(k - 1 < NPAY)
+        def _():
+            r4(k - 1)
 
         @pl.when(c >= 1)
         def _():
             reduce_grads(c - 1)
 
-        @pl.when(c == NCH - 1)
-        def _():
-            igs[...] = ig[pl.ds(theirs, HALF), :].astype(BF)
-
         main_tile(c, 2)
 
-        @pl.when(c == NCH - 1)
-        def _():
-            ig_pair.start()
-
-        @pl.when(p < NPAY)
-        def _():
-            r4(p)
-
-        @pl.when(c >= 2)
-        def _():
-            finish_grads(c - 2)
+        @pl.when(k + 2 < NPAY)
+        def _():
+            r0(k + 2)
 
         @pl.when(c == 1)
         def _():
@@ -427,26 +415,38 @@
         def _():
             send_down_sq()
 
+        main_grads()
         send_grads(c)
+        main_input(c)
         return carry
 
     lax.fori_loop(0, NCH, chunk, 0)
 
-    finish_grads(NCH - 2)
+    igs[...] = ig[pl.ds(theirs, HALF), :].astype(BF)
+    mine_part = ig[pl.ds(mine, HALF), :].astype(BF).astype(F32)
+    ig[pl.ds(mine, HALF), :] = mine_part
+    ig_pair.start()
+    reduce_grads(NCH - 1)
+    sqs[...] = jnp.sum(sqacc[...].T, axis=0, keepdims=True)
+    sqr[rep * 2 + fs] = sqs[...]
+    for d in range(1, 8):
+        other = {"rep": (rep + d // 2) % 4, "fs": (fs + d) % 2}
+        pltpu.make_async_remote_copy(
+            src_ref=sqs,
+            dst_ref=sqr.at[rep * 2 + fs],
+            send_sem=r_send.at[3],
+            recv_sem=r_recv.at[3],
+            device_id=other,
+            device_id_type=MESH,
+        ).start()
     ig_pair.wait_recv()
-    mine_part = ig[pl.ds(mine, HALF), :].astype(BF).astype(F32)
-    ig_out[...] = (mine_part + igr[...].astype(F32)).astype(BF)
-    reduce_grads(NCH - 1)
+    ig_out[...] = (ig[pl.ds(mine, HALF), :] + igr[...].astype(F32)).astype(BF)
     all15 = dsqr.at[pl.ds(0, 15)]
     pltpu.make_async_copy(all15, all15, q_recv).wait()
     total = dsqr[0]
     for k in range(1, 16):
         total = total + dsqr[k]
     dsq_out[...] = total
-    finish_grads(NCH - 1)
-    sqs[...] = jnp.sum(sqacc[...].T, axis=0, keepdims=True)
-    sq_pair = d2d(sqs, sqr, 3)
-    sq_pair.start()
 
     for p in range(NPAY):
         take(send_sem.at[p], 15)
@@ -461,10 +461,32 @@
     cot_pair.wait_send()
     x_pair.wait_send()
     ig_pair.wait_send()
-    sq_pair.wait()
-    both_sq = sqs[...] + sqr[...]
-    gsq_out[...] = both_sq[:, 0:128]
-    usq_out[...] = both_sq[:, 128:256]
+    for k in range(NCH):
+        three(ag.at[k], ag_recv.at[k])
+    all7 = sqr.at[pl.ds(0, 7)]
+    pltpu.make_async_copy(all7, all7, r_send.at[3]).wait()
+    pltpu.make_async_copy(all7, all7, r_recv.at[3]).wait()
+    total = sqr[0]
+    for k in range(1, 8):
+        total = total + sqr[k]
+    sq_out[...] = total
+
+
+def finish(ig, ag, dag, sq, dsq, ig_out, gg_out, ug_out, dg_out, gsq_out, usq_out, dsq_out):
+    ig_out[...] = ig[...]
+    for c in range(NCH):
+        for j in range(4):
+            v = ag[c, j].astype(F32)
+            gg_out[32 * j : 32 * j + 32, c * CH : (c + 1) * CH] = v[0:32]
+            ug_out[32 * j : 32 * j + 32, c * CH : (c + 1) * CH] = v[32:64]
+    for k in range(FH // 128):
+        v = jnp.concatenate(
+            [dag[j, :, 128 * k : 128 * k + 128].astype(F32) for j in range(4)], axis=0
+        )
+        dg_out[128 * k : 128 * k + 128, :] = v.T
+    gsq_out[...] = sq[0, 0:128]
+    usq_out[...] = sq[0, 128:256]
+    dsq_out[...] = dsq[0, :]
 
 
 def on_device(layer_input, cotangent, gate_pre, up_pre, gate_weight, up_weight, down_weight):
@@ -475,15 +497,13 @@
         body,
         out_shape=(
             jax.ShapeDtypeStruct((HALF, 128), BF),
-            jax.ShapeDtypeStruct((128, FH), F32),
-            jax.ShapeDtypeStruct((128, FH), F32),
-            jax.ShapeDtypeStruct((FH, 128), F32),
-            jax.ShapeDtypeStruct((1, 128), F32),
-            jax.ShapeDtypeStruct((1, 128), F32),
+            jax.ShapeDtypeStruct((NCH, 4, 64, CH), BF),
+            jax.ShapeDtypeStruct((4, 32, FH), BF),
+            jax.ShapeDtypeStruct((1, 256), F32),
             jax.ShapeDtypeStruct((1, FH), F32),
         ),
         in_specs=[anyspec] * 7,
-        out_specs=(vm,) * 7,
+        out_specs=(vm,) * 5,
         scratch_shapes=[
             pltpu.VMEM((16, TOK + FH, 128), BF),
             pltpu.VMEM((NCH, TOK, CH), BF),
@@ -492,23 +512,22 @@
             pltpu.VMEM((2, TP, FH), BF),
             pltpu.VMEM((TP, FH), BF),
             pltpu.VMEM((TOK, 128), BF),
-            pltpu.VMEM((4, 128, TM), BF),
+            pltpu.VMEM((128, TOK), BF),
             pltpu.VMEM((128, FH), F32),
             pltpu.VMEM((TOK, 128), F32),
             pltpu.VMEM((128, FH), BF),
             pltpu.VMEM((128, FH), BF),
+            pltpu.VMEM((TOK, 2 * CH), BF),
             pltpu.VMEM((128, 2 * CH), F32),
             pltpu.VMEM((NCH, 4, 64, CH), BF),
             pltpu.VMEM((NCH, 4, 64, CH), BF),
-            pltpu.VMEM((NCH, 4, 64, CH), BF),
-            pltpu.VMEM((4, 32, FH), BF),
             pltpu.VMEM((4, 32, FH), BF),
             pltpu.VMEM((4, 32, FH), BF),
             pltpu.VMEM((HALF, 128), BF),
             pltpu.VMEM((HALF, 128), BF),
             pltpu.VMEM((256, 128), F32),
             pltpu.VMEM((1, 256), F32),
-            pltpu.VMEM((1, 256), F32),
+            pltpu.VMEM((8, 1, 256), F32),
             pltpu.VMEM((1, FH), F32),
             pltpu.VMEM((16, 1, FH), F32),
             dma((NPAY,)),
@@ -531,8 +550,21 @@
         ),
         name="backward",
     )(layer_input, cotangent, gate_pre, up_pre, gate_weight, up_weight, down_weight)
-    ig, gg, ug, dg, gsq, usq, dsq = outs
-    return ig, gg, ug, dg, gsq.reshape(128), usq.reshape(128), dsq.reshape(FH)
+    return pl.pallas_call(
+        finish,
+        out_shape=(
+            jax.ShapeDtypeStruct((HALF, 128), BF),
+            jax.ShapeDtypeStruct((128, FH), F32),
+            jax.ShapeDtypeStruct((128, FH), F32),
+            jax.ShapeDtypeStruct((FH, 128), F32),
+            jax.ShapeDtypeStruct((128,), F32),
+            jax.ShapeDtypeStruct((128,), F32),
+            jax.ShapeDtypeStruct((FH,), F32),
+        ),
+        in_specs=[vm] * 5,
+        out_specs=(vm,) * 7,
+        name="outputs",
+    )(*outs)
 
 
 def solution(mesh):

time: 140 us -> 122 us (0.87)
  local copies, waits for them, and re-layouts: 10.3 us -> 0 us
  Pallas kernels: 127 us -> 121 us
    unnamed x6 -> x0, local copies, waits for them, and re-layouts: 10.3 us -> none
    pallas_call x1, Pallas kernels: 127 us -> 118 us  [on_device(): pl.pallas_call(body, out_shape=(jax.ShapeDtypeStruct((HALF, 128), BF), ja...]
    pallas_call x0 -> x1, Pallas kernels: none -> 3.03 us  [on_device(): pl.pallas_call(finish, out_shape=(jax.ShapeDtypeStruct((HALF, 128), BF),...]
where the time goes in v2:
time: 122 us
  Pallas kernels  121 us (99%)
    pallas_call x1, Pallas kernels, on_device(): pl.pallas_call(body, out_shape=(jax.ShapeDtypeStruct((HALF, 128), BF), ja...  118 us
    pallas_call x1, Pallas kernels, on_device(): pl.pallas_call(finish, out_shape=(jax.ShapeDtypeStruct((HALF, 128), BF),...  3.03 us

profile of v2, /device:TPU:1, one launch (start us, length us, event | category | flops | bytes accessed | tf_op | source)
XLA Modules:
  0.0 121.6 jit_solution(686124181493260497)
XLA Ops:
  0.6 117.9 %backward.1 = (bf16[1280,128]{1,0:T(8,128)(2,1)}, bf16[6,4,64,256]{3,2,1,0:T(8,128)(2,1)}, bf16[4,32,1536]{2,1,0:T(8,128)(2,1)}, f32[1,256]{1,0:T(1,128)}, f32[1,1536]{1,0:T(1,128)}) custom-call(bf16[1280,128]{1,0:T(8,128)(2,1)} %x_hbm.1, bf16[1280,128]{1,0:T(8,128)(2,1)} %cot_hbm.1, bf16[2560,1536]{1,0:T(8,128)(2,1)} %gate_hbm.1, ...), custom_call_target="tpu_custom_call" | custom-call | tf_op jit(solution)/shard_map/backward/pallas_call | solution.py:496
  118.6 3.0 %outputs.1 = (bf16[1280,128]{1,0:T(8,128)(2,1)}, f32[128,1536]{1,0:T(8,128)}, f32[128,1536]{1,0:T(8,128)}, f32[1536,128]{1,0:T(8,128)}, f32[128]{0:T(128)}, /*index=5*/f32[128]{0:T(128)}, f32[1536]{0:T(1024)}) custom-call(bf16[1280,128]{1,0:T(8,128)(2,1)} %get-tuple-element.12.ig, bf16[6,4,64,256]{3,2,1,0:T(8,128)(2,1)} %get-tuple-element.13.ag, ...), custom_call_target="tpu_custom_call" | custom-call | tf_op jit(solution)/shard_map/outputs/pallas_call | solution.py:553

commit v3 on v2

--- a/solution.py
+++ b/solution.py
@@ -27,7 +27,7 @@
     x_hbm, cot_hbm, gate_hbm, up_hbm, gw_hbm, uw_hbm, dw_hbm,
     ig_out, ag, dag, sq_out, dsq_out,
     allb, aa, cc, gbuf, ubuf, hid, xb, xt, dgt, ig, gw, uw,
-    gb, gacc, gs, rs, ds, dr, igs, igr, sqacc, sqs, sqr, dsqs, dsqr,
+    gb, wt, gacc, gs, rs, ds, dr, igs, igr, sqacc, sqs, sqr, dsqs, dsqr,
     send_sem, recv_sem, d2d_send, d2d_recv, loc_sem, tile_sem,
     rs_send, rs_recv, ag_send, ag_recv, q_send, q_recv, r_send, r_recv,
 ):
@@ -180,6 +180,7 @@
     own_cot.wait()
     r0(0)
     r0(1)
+    r0(2)
     cot_pair = d2d(allb.at[tp, pl.ds(mine, HALF)], allb.at[tp, pl.ds(mine, HALF)], 0)
     cot_pair.start()
     own_x.wait()
@@ -243,7 +244,7 @@
         def _():
             r4(k - 1)
 
-        r0(k + 2)
+        r0(k + 3)
         tile(2 * k + 1)
 
         @pl.when(k >= 2)
@@ -293,22 +294,24 @@
         if k == NCOT:
             scatter(ds, dr, rs_send.at[NCH], rs_recv.at[NCH])
         r4(k - 1)
-        r0(k + 2)
+        r0(k + 3)
         r5(k - 2)
         to_sibling(k - 2)
     for k in range(NCOT):
         take(d2d_recv.at[k], 15)
 
+    def main_weight(c):
+        fr = pl.ds(pl.multiple_of(TOK + c * CH, CH), CH)
+        for k in range(16):
+            wt[128 * k : 128 * k + 128, :] = allb[k, fr, :].astype(F32).T.astype(BF)
+
     def main_tile(c, j):
-        rows = pl.ds(j * TM, TM)
-        fr = pl.ds(pl.multiple_of(TOK + c * CH, CH), CH)
-        lhs = jnp.concatenate([allb[k, rows, :] for k in range(16)], axis=1)
-        rhs = jnp.concatenate([allb[k, fr, :] for k in range(16)], axis=1)
-        hg = lax.dot_general(lhs, rhs, (((1,), (1,)), ((), ())), preferred_element_type=F32)
-        gd = (hg * cc[c, rows, :].astype(F32)).astype(BF)
-        ud = (hg * aa[c, rows, :].astype(F32)).astype(BF)
-        gb[rows, 0:CH] = gd
-        gb[rows, CH : 2 * CH] = ud
+        for i in range(2):
+            rows = pl.ds(j * TM + i * (TM // 2), TM // 2)
+            lhs = jnp.concatenate([allb[k, rows, :] for k in range(16)], axis=1)
+            hg = jnp.dot(lhs, wt[...], preferred_element_type=F32)
+            gb[rows, 0:CH] = (hg * cc[c, rows, :].astype(F32)).astype(BF)
+            gb[rows, CH : 2 * CH] = (hg * aa[c, rows, :].astype(F32)).astype(BF)
 
     def main_grads():
         gacc[...] = jnp.dot(xt[...], gb[...], preferred_element_type=F32)
@@ -332,11 +335,11 @@
         v = rs[c, 0].astype(F32) + rs[c, 1].astype(F32)
         v = v + rs[c, 2].astype(F32) + rs[c, 3].astype(F32)
         ag[c, rep] = v.astype(BF)
-        spread(ag.at[c], ag_send.at[c], ag_recv.at[c])
         w = v * v
         w = w[:, 0:128] + w[:, 128:256]
         sqacc[pl.ds(pl.multiple_of(32 * rep, 32), 32), :] += w[0:32]
         sqacc[pl.ds(pl.multiple_of(128 + 32 * rep, 32), 32), :] += w[32:64]
+        spread(ag.at[c], ag_send.at[c], ag_recv.at[c])
 
     def reduce_down():
         three(dr, rs_recv.at[NCH])
@@ -379,6 +382,7 @@
             r1(k + 1)
 
         r5(k - 2)
+        main_weight(c)
         main_tile(c, 0)
 
         @pl.when(k < NPAY)
@@ -395,25 +399,25 @@
         def _():
             r4(k - 1)
 
+        main_tile(c, 2)
+
+        @pl.when(k + 3 < NPAY)
+        def _():
+            r0(k + 3)
+
+        @pl.when(c == 1)
+        def _():
+            finish_down()
+
+        main_tile(c, 3)
+
+        @pl.when(c == 1)
+        def _():
+            send_down_sq()
+
         @pl.when(c >= 1)
         def _():
             reduce_grads(c - 1)
-
-        main_tile(c, 2)
-
-        @pl.when(k + 2 < NPAY)
-        def _():
-            r0(k + 2)
-
-        @pl.when(c == 1)
-        def _():
-            finish_down()
-
-        main_tile(c, 3)
-
-        @pl.when(c == 1)
-        def _():
-            send_down_sq()
 
         main_grads()
         send_grads(c)
@@ -518,6 +522,7 @@
             pltpu.VMEM((128, FH), BF),
             pltpu.VMEM((128, FH), BF),
             pltpu.VMEM((TOK, 2 * CH), BF),
+            pltpu.VMEM((2048, CH), BF),
             pltpu.VMEM((128, 2 * CH), F32),
             pltpu.VMEM((NCH, 4, 64, CH), BF),
             pltpu.VMEM((NCH, 4, 64, CH), BF),

time: 122 us -> 99.1 us (0.81)
  Pallas kernels: 121 us -> 98.4 us
    pallas_call x1, Pallas kernels: 118 us -> 95.3 us  [on_device(): pl.pallas_call(body, out_shape=(jax.ShapeDtypeStruct((HALF, 128), BF), ja...]
where the time goes in v3:
time: 99.1 us; the launch traced here: 99 us
  Pallas kernels  98.4 us (99%)
    pallas_call x1, Pallas kernels, on_device(): pl.pallas_call(body, out_shape=(jax.ShapeDtypeStruct((HALF, 128), BF), ja...  95.3 us
    pallas_call x1, Pallas kernels, on_device(): pl.pallas_call(finish, out_shape=(jax.ShapeDtypeStruct((HALF, 128), BF),...  3.03 us

profile of v3, /device:TPU:1, one launch (start us, length us, event | category | flops | bytes accessed | tf_op | source)
XLA Modules:
  0.0 99.0 jit_solution(18293851688580785993)
XLA Ops:
  0.6 95.3 %backward.1 = (bf16[1280,128]{1,0:T(8,128)(2,1)}, bf16[6,4,64,256]{3,2,1,0:T(8,128)(2,1)}, bf16[4,32,1536]{2,1,0:T(8,128)(2,1)}, f32[1,256]{1,0:T(1,128)}, f32[1,1536]{1,0:T(1,128)}) custom-call(bf16[1280,128]{1,0:T(8,128)(2,1)} %x_hbm.1, bf16[1280,128]{1,0:T(8,128)(2,1)} %cot_hbm.1, bf16[2560,1536]{1,0:T(8,128)(2,1)} %gate_hbm.1, ...), custom_call_target="tpu_custom_call" | custom-call | tf_op jit(solution)/shard_map/backward/pallas_call | solution.py:500
  96.0 3.0 %outputs.1 = (bf16[1280,128]{1,0:T(8,128)(2,1)}, f32[128,1536]{1,0:T(8,128)}, f32[128,1536]{1,0:T(8,128)}, f32[1536,128]{1,0:T(8,128)}, f32[128]{0:T(128)}, /*index=5*/f32[128]{0:T(128)}, f32[1536]{0:T(1024)}) custom-call(bf16[1280,128]{1,0:T(8,128)(2,1)} %get-tuple-element.12.ig, bf16[6,4,64,256]{3,2,1,0:T(8,128)(2,1)} %get-tuple-element.13.ag, ...), custom_call_target="tpu_custom_call" | custom-call | tf_op jit(solution)/shard_map/outputs/pallas_call | solution.py:558

commit v4 on v3

--- a/solution.py
+++ b/solution.py
@@ -18,7 +18,9 @@
 CH = 256
 NCH = FH // CH
 NCOT = HALF // N
-NPAY = NCOT + NCH
+SH = CH // 4
+NXC = 2
+NPAY = NCOT + NCH - NXC
 TM = 640
 TP = 256
 
@@ -27,8 +29,8 @@
     x_hbm, cot_hbm, gate_hbm, up_hbm, gw_hbm, uw_hbm, dw_hbm,
     ig_out, ag, dag, sq_out, dsq_out,
     allb, aa, cc, gbuf, ubuf, hid, xb, xt, dgt, ig, gw, uw,
-    gb, wt, gacc, gs, rs, ds, dr, igs, igr, sqacc, sqs, sqr, dsqs, dsqr,
-    send_sem, recv_sem, d2d_send, d2d_recv, loc_sem, tile_sem,
+    wt, gacc, gs, rs, ds, dr, igs, igr, sqacc, sqs, sqr, dsqs, dsqr,
+    send_sem, recv_sem, x_send, x_recv, d2d_send, d2d_recv, loc_sem, tile_sem,
     rs_send, rs_recv, ag_send, ag_recv, q_send, q_recv, r_send, r_recv,
 ):
     rep = lax.axis_index("rep")
@@ -45,13 +47,22 @@
     theirs = pl.multiple_of(sib * HALF, HALF)
 
     own_cot = pltpu.make_async_copy(cot_hbm, allb.at[tp, pl.ds(mine, HALF)], loc_sem.at[0])
-    own_dw = pltpu.make_async_copy(dw_hbm, allb.at[tp, pl.ds(TOK, FH)], loc_sem.at[1])
+    own_rows = [(CH * i + SH * rep, SH, 5 + i) for i in range(NXC)] + [(NXC * CH, FH - NXC * CH, 1)]
+    own_dw = [
+        pltpu.make_async_copy(
+            dw_hbm.at[pl.ds(pl.multiple_of(r, SH), n)],
+            allb.at[tp, pl.ds(pl.multiple_of(TOK + r, SH), n)],
+            loc_sem.at[k],
+        )
+        for r, n, k in own_rows
+    ]
     own_x = pltpu.make_async_copy(x_hbm, xb.at[pl.ds(mine, HALF)], loc_sem.at[2])
     own_gw = pltpu.make_async_copy(gw_hbm, gw, loc_sem.at[3])
     own_uw = pltpu.make_async_copy(uw_hbm, uw, loc_sem.at[4])
     own_cot.start()
     own_x.start()
-    own_dw.start()
+    for c in own_dw:
+        c.start()
 
     def tile_rows(i):
         return pl.multiple_of(((fs * 5 + i) % 10) * TP, TP)
@@ -83,10 +94,18 @@
 
     def row0(p):
         w = (p + 11) // 16
-        return 256 * p + HALF * (w + fs * (1 - w))
-
-    def put(p, b, off, n, dz, dy, g):
-        rows = pl.ds(pl.multiple_of(row0(p) + off, 64), n)
+        return 256 * p + w * (NXC * CH + HALF) + (1 - w) * fs * HALF
+
+    def whole(p):
+        return p, row0(p), N
+
+    def share(i):
+        return NPAY + i, TOK + CH * i + SH * rep, SH
+
+    def put(pay, b, first, num, dz, dy, g):
+        p, row, n = pay
+        q = n // 4
+        rows = pl.ds(pl.multiple_of(row + first * q, 16), num * q)
         ref = allb.at[b, rows]
         pltpu.make_async_remote_copy(
             src_ref=ref,
@@ -97,67 +116,83 @@
             device_id_type=MESH,
         ).start()
 
-    def take(sem, k):
-        ref = allb.at[pl.ds(0, k), pl.ds(0, N)]
+    def take(sem, k, n=N):
+        ref = allb.at[pl.ds(0, k), pl.ds(0, n)]
         pltpu.make_async_copy(ref, ref, sem).wait()
 
-    H, Q = N // 2, N // 4
-    OA, OB = 0, H
-
-    def both_y(p, b, g):
-        put(p, b, OA, H, 0, 1, g)
-        put(p, b, OA, H, 0, -1, g)
-
-    def both_z(p, b, g):
-        put(p, b, OB, H, 1, 0, g)
-        put(p, b, OB, H, -1, 0, g)
-
-    def r0(p):
-        put(p, tp, OA, H, 1, 0, 0)
-        put(p, tp, OA, H, -1, 0, 0)
-        put(p, tp, OB, H, 0, 1, 0)
-        put(p, tp, OB, H, 0, -1, 0)
-        both_y(p, tp, 2)
-        both_z(p, tp, 2)
-
-    def r1(p):
-        take(recv_sem.at[p, 0], 2)
-        put(p, blk(-1, 0), OA, Q, 1, 0, 1)
-        put(p, blk(1, 0), OA + Q, Q, -1, 0, 1)
-        put(p, blk(0, -1), OB, Q, 0, 1, 1)
-        put(p, blk(0, 1), OB + Q, Q, 0, -1, 1)
+    def got(pay, g, k):
+        take(recv_sem.at[pay[0], g], k, pay[2])
+
+    def both_y(pay, b, g):
+        put(pay, b, 0, 2, 0, 1, g)
+        put(pay, b, 0, 2, 0, -1, g)
+
+    def both_z(pay, b, g):
+        put(pay, b, 2, 2, 1, 0, g)
+        put(pay, b, 2, 2, -1, 0, g)
+
+    def r0(pay):
+        put(pay, tp, 0, 2, 1, 0, 0)
+        put(pay, tp, 0, 2, -1, 0, 0)
+        put(pay, tp, 2, 2, 0, 1, 0)
+        put(pay, tp, 2, 2, 0, -1, 0)
+        both_y(pay, tp, 2)
+        both_z(pay, tp, 2)
+
+    def r1(pay):
+        got(pay, 0, 2)
+        put(pay, blk(-1, 0), 0, 1, 1, 0, 1)
+        put(pay, blk(1, 0), 1, 1, -1, 0, 1)
+        put(pay, blk(0, -1), 2, 1, 0, 1, 1)
+        put(pay, blk(0, 1), 3, 1, 0, -1, 1)
         for d in (-1, 1):
-            both_y(p, blk(d, 0), 2)
-            both_z(p, blk(0, d), 2)
-
-    def r2(p):
-        take(recv_sem.at[p, 1], 1)
-        both_y(p, blk(2, 0), 3)
-        both_z(p, blk(0, 2), 3)
-
-    def onward(p, d, g):
-        put(p, blk(d, -1), OA, Q, 0, 1, g)
-        put(p, blk(d, 1), OA + Q, Q, 0, -1, g)
-        put(p, blk(-1, d), OB, Q, 1, 0, g)
-        put(p, blk(1, d), OB + Q, Q, -1, 0, g)
-
-    def r3(p):
-        take(recv_sem.at[p, 2], 6)
+            both_y(pay, blk(d, 0), 2)
+            both_z(pay, blk(0, d), 2)
+
+    def r2(pay):
+        got(pay, 1, 1)
+        both_y(pay, blk(2, 0), 3)
+        both_z(pay, blk(0, 2), 3)
+
+    def onward(pay, d, g):
+        put(pay, blk(d, -1), 0, 1, 0, 1, g)
+        put(pay, blk(d, 1), 1, 1, 0, -1, g)
+        put(pay, blk(-1, d), 2, 1, 1, 0, g)
+        put(pay, blk(1, d), 3, 1, -1, 0, g)
+
+    def r3(pay):
+        got(pay, 2, 6)
         for d in (0, -1, 1):
-            onward(p, d, 4)
-
-    def r4(p):
-        take(recv_sem.at[p, 3], 2)
-        onward(p, 2, 5)
-
-    def r5(p):
-        take(recv_sem.at[p, 4], 3)
-        take(recv_sem.at[p, 5], 1)
-
-    def to_sibling(p):
+            onward(pay, d, 4)
+
+    def r4(pay):
+        got(pay, 3, 2)
+        onward(pay, 2, 5)
+
+    def r5(pay):
+        got(pay, 4, 3)
+        got(pay, 5, 1)
+
+    def over_rep(i):
+        rows = pl.ds(pl.multiple_of(TOK + CH * i + SH * rep, SH), SH)
+        ref = allb.at[pl.ds(0, 16), rows]
+        for d in (1, 3, 2):
+            pltpu.make_async_remote_copy(
+                src_ref=ref,
+                dst_ref=ref,
+                send_sem=x_send.at[i],
+                recv_sem=x_recv.at[i],
+                device_id={"rep": (rep + d) % 4},
+                device_id_type=MESH,
+            ).start()
+
+    NEAR = [(dz, dy) for dz in (0, 1, -1) for dy in (0, 1, -1) if (dz, dy) != (0, 0)]
+    FAR = [(2, dy) for dy in (0, 1, -1, 2)] + [(dz, 2) for dz in (0, 1, -1)]
+
+    def to_sibling(p, blocks):
         rows = pl.ds(pl.multiple_of(fs * HALF + N * p, N), N)
-        for d in range(1, 16):
-            ref = allb.at[(tp + d) % 16, rows]
+        for dz, dy in blocks:
+            ref = allb.at[blk(dz, dy), rows]
             pltpu.make_async_remote_copy(
                 src_ref=ref,
                 dst_ref=ref,
@@ -177,22 +212,27 @@
             device_id_type=MESH,
         )
 
+    for c in own_dw:
+        c.wait()
+    shares = [share(i) for i in range(NXC)]
+    for h in shares:
+        r0(h)
     own_cot.wait()
-    r0(0)
-    r0(1)
-    r0(2)
+    r0(whole(0))
+    r0(whole(1))
     cot_pair = d2d(allb.at[tp, pl.ds(mine, HALF)], allb.at[tp, pl.ds(mine, HALF)], 0)
     cot_pair.start()
     own_x.wait()
     x_pair = d2d(xb.at[pl.ds(mine, HALF)], xb.at[pl.ds(mine, HALF)], 1)
     x_pair.start()
-    own_dw.wait()
     own_gw.wait()
     own_uw.wait()
     dgt[...] = jnp.zeros_like(dgt)
-    ig[...] = jnp.zeros_like(ig)
     sqacc[...] = jnp.zeros_like(sqacc)
-    r1(0)
+    for h in shares:
+        r1(h)
+    r0(whole(2))
+    r1(whole(0))
     cot_pair.wait_recv()
     x_pair.wait_recv()
 
@@ -202,7 +242,16 @@
         xt[:, pl.ds(r, 128)] = v.T.astype(BF)
         return carry
 
+    for h in shares:
+        r2(h)
+    for h in shares:
+        r3(h)
+    r0(whole(3))
+    r1(whole(1))
     lax.fori_loop(0, TOK // 128, transpose_x, 0)
+    for h in shares:
+        r4(h)
+    r0(whole(4))
 
     def tile(i):
         slot = i % 2
@@ -235,26 +284,37 @@
         dgt[...] += jnp.dot(ct, hid[...], preferred_element_type=F32)
 
     def first(k, carry):
-        r2(k)
-        r1(k + 1)
+        r2(whole(k))
+
+        @pl.when(k + 2 < NCOT)
+        def _():
+            r1(whole(k + 2))
+
         tile(2 * k)
-        r3(k)
+
+        @pl.when(k == 0)
+        def _():
+            for i, h in enumerate(shares):
+                r5(h)
+                over_rep(i)
+
+        r3(whole(k))
+        to_sibling(k, NEAR)
 
         @pl.when(k >= 1)
         def _():
-            r4(k - 1)
-
-        r0(k + 3)
+            r4(whole(k - 1))
+
         tile(2 * k + 1)
 
         @pl.when(k >= 2)
         def _():
-            r5(k - 2)
-            to_sibling(k - 2)
+            r5(whole(k - 2))
+            to_sibling(k - 2, FAR)
 
         return carry
 
-    lax.fori_loop(0, NCOT, first, 0)
+    lax.fori_loop(0, NCOT - 1, first, 0)
 
     def scatter(src, dst, s_sem, r_sem):
         for d in range(1, 4):
@@ -283,20 +343,29 @@
         ref = buf.at[pl.ds(0, 3)]
         pltpu.make_async_copy(ref, ref, sem).wait()
 
-    for k in range(NCOT, NCOT + 2):
-        r2(k)
-        r1(k + 1)
-        if k == NCOT:
-            for j in range(4):
-                ds[j] = (dgt[32 * j : 32 * j + 32, :] * scale).astype(BF)
-            dr[rep] = ds[rep]
-        r3(k)
-        if k == NCOT:
-            scatter(ds, dr, rs_send.at[NCH], rs_recv.at[NCH])
-        r4(k - 1)
-        r0(k + 3)
-        r5(k - 2)
-        to_sibling(k - 2)
+    k = NCOT - 1
+    r2(whole(k))
+    tile(2 * k)
+    r3(whole(k))
+    to_sibling(k, NEAR)
+    r4(whole(k - 1))
+    r0(whole(k + 1))
+    tile(2 * k + 1)
+    r5(whole(k - 2))
+    to_sibling(k - 2, FAR)
+    for j in range(4):
+        ds[j] = (dgt[32 * j : 32 * j + 32, :] * scale).astype(BF)
+    dr[rep] = ds[rep]
+    r4(whole(k))
+    r5(whole(k - 1))
+    to_sibling(k - 1, FAR)
+    r0(whole(k + 2))
+    r1(whole(k + 1))
+    scatter(ds, dr, rs_send.at[NCH], rs_recv.at[NCH])
+    r5(whole(k))
+    to_sibling(k, FAR)
+    r0(whole(k + 3))
+    take(x_recv.at[0], 12)
     for k in range(NCOT):
         take(d2d_recv.at[k], 15)
 
@@ -310,18 +379,26 @@
             rows = pl.ds(j * TM + i * (TM // 2), TM // 2)
             lhs = jnp.concatenate([allb[k, rows, :] for k in range(16)], axis=1)
             hg = jnp.dot(lhs, wt[...], preferred_element_type=F32)
-            gb[rows, 0:CH] = (hg * cc[c, rows, :].astype(F32)).astype(BF)
-            gb[rows, CH : 2 * CH] = (hg * aa[c, rows, :].astype(F32)).astype(BF)
-
-    def main_grads():
-        gacc[...] = jnp.dot(xt[...], gb[...], preferred_element_type=F32)
-
-    def main_input(c):
-        cols = pl.ds(pl.multiple_of(c * CH, CH), CH)
-        wts = jnp.concatenate([gw[:, cols], uw[:, cols]], axis=1)
-        ig[...] += lax.dot_general(
-            gb[...], wts, (((1,), (1,)), ((), ())), preferred_element_type=F32
-        )
+            cc[c, rows, :] = (hg * cc[c, rows, :].astype(F32)).astype(BF)
+            aa[c, rows, :] = (hg * aa[c, rows, :].astype(F32)).astype(BF)
+
+    def main_grads(c):
+        gacc[:, 0:CH] = jnp.dot(xt[...], cc[c], preferred_element_type=F32)
+        gacc[:, CH : 2 * CH] = jnp.dot(xt[...], aa[c], preferred_element_type=F32)
+
+    def input_part(start):
+        wts = jnp.concatenate([gw[...], uw[...]], axis=1)
+        parts = []
+        for i in range(2):
+            rows = pl.ds(pl.multiple_of(start + i * TM, TM), TM)
+            lhs = jnp.concatenate(
+                [cc[c, rows, :] for c in range(NCH)] + [aa[c, rows, :] for c in range(NCH)],
+                axis=1,
+            )
+            parts.append(
+                lax.dot_general(lhs, wts, (((1,), (1,)), ((), ())), preferred_element_type=F32)
+            )
+        return parts
 
     def send_grads(c):
         for j in range(4):
@@ -371,66 +448,72 @@
     ig_pair = d2d(igs, igr, 2)
 
     def chunk(c, carry):
-        k = NCOT + 2 + c
-
-        @pl.when(k < NPAY)
-        def _():
-            r2(k)
-
-        @pl.when(k + 1 < NPAY)
-        def _():
-            r1(k + 1)
-
-        r5(k - 2)
+        k = NCOT + c
+
+        @pl.when(c == 1)
+        def _():
+            take(x_recv.at[1], 12)
+
         main_weight(c)
         main_tile(c, 0)
 
+        @pl.when((c >= 1) & (k - 1 < NPAY))
+        def _():
+            r4(whole(k - 1))
+
+        @pl.when(c == 0)
+        def _():
+            r0(whole(NPAY - 1))
+
+        main_tile(c, 1)
+
         @pl.when(k < NPAY)
         def _():
-            r3(k)
-
-        @pl.when(c == 0)
+            r2(whole(k))
+
+        @pl.when(k + 1 < NPAY)
+        def _():
+            r1(whole(k + 1))
+
+        main_tile(c, 2)
+
+        @pl.when(k < NPAY)
+        def _():
+            r3(whole(k))
+
+        @pl.when(c == 2)
         def _():
             reduce_down()
 
-        main_tile(c, 1)
-
-        @pl.when(k - 1 < NPAY)
-        def _():
-            r4(k - 1)
-
-        main_tile(c, 2)
-
-        @pl.when(k + 3 < NPAY)
-        def _():
-            r0(k + 3)
-
-        @pl.when(c == 1)
+        @pl.when(c == 4)
         def _():
             finish_down()
 
         main_tile(c, 3)
 
-        @pl.when(c == 1)
+        @pl.when(c == 4)
         def _():
             send_down_sq()
 
-        @pl.when(c >= 1)
-        def _():
-            reduce_grads(c - 1)
-
-        main_grads()
+        @pl.when(c >= 2)
+        def _():
+            reduce_grads(c - 2)
+
+        @pl.when((c >= 1) & (k - 1 < NPAY))
+        def _():
+            r5(whole(k - 1))
+
+        main_grads(c)
         send_grads(c)
-        main_input(c)
         return carry
 
     lax.fori_loop(0, NCH, chunk, 0)
 
-    igs[...] = ig[pl.ds(theirs, HALF), :].astype(BF)
-    mine_part = ig[pl.ds(mine, HALF), :].astype(BF).astype(F32)
-    ig[pl.ds(mine, HALF), :] = mine_part
+    reduce_grads(NCH - 2)
+    for i, v in enumerate(input_part(theirs)):
+        igs[i * TM : (i + 1) * TM, :] = v.astype(BF)
+    reduce_grads(NCH - 1)
     ig_pair.start()
-    reduce_grads(NCH - 1)
     sqs[...] = jnp.sum(sqacc[...].T, axis=0, keepdims=True)
     sqr[rep * 2 + fs] = sqs[...]
     for d in range(1, 8):
@@ -443,8 +526,10 @@
             device_id=other,
             device_id_type=MESH,
         ).start()
+    for i, v in enumerate(input_part(mine)):
+        ig[i * TM : (i + 1) * TM, :] = v.astype(BF).astype(F32)
     ig_pair.wait_recv()
-    ig_out[...] = (ig[pl.ds(mine, HALF), :] + igr[...].astype(F32)).astype(BF)
+    ig_out[...] = (ig[...] + igr[...].astype(F32)).astype(BF)
     all15 = dsqr.at[pl.ds(0, 15)]
     pltpu.make_async_copy(all15, all15, q_recv).wait()
     total = dsqr[0]
@@ -454,6 +539,9 @@
 
     for p in range(NPAY):
         take(send_sem.at[p], 15)
+    for i in range(NXC):
+        take(send_sem.at[NPAY + i], 15, SH)
+        take(x_send.at[i], 12)
     for k in range(NCOT):
         take(d2d_send.at[k], 15)
     for k in range(NCH):
@@ -518,10 +606,9 @@
             pltpu.VMEM((TOK, 128), BF),
             pltpu.VMEM((128, TOK), BF),
             pltpu.VMEM((128, FH), F32),
-            pltpu.VMEM((TOK, 128), F32),
+            pltpu.VMEM((HALF, 128), F32),
             pltpu.VMEM((128, FH), BF),
             pltpu.VMEM((128, FH), BF),
-            pltpu.VMEM((TOK, 2 * CH), BF),
             pltpu.VMEM((2048, CH), BF),
             pltpu.VMEM((128, 2 * CH), F32),
             pltpu.VMEM((NCH, 4, 64, CH), BF),
@@ -535,11 +622,13 @@
             pltpu.VMEM((8, 1, 256), F32),
             pltpu.VMEM((1, FH), F32),
             pltpu.VMEM((16, 1, FH), F32),
-            dma((NPAY,)),
-            dma((NPAY, 6)),
+            dma((NPAY + NXC,)),
+            dma((NPAY + NXC, 6)),
+            dma((NXC,)),
+            dma((NXC,)),
             dma((NCOT,)),
             dma((NCOT,)),
-            dma((5,)),
+            dma((5 + NXC,)),
             dma((2, 2)),
             dma((NCH + 1,)),
             dma((NCH + 1,)),

time: 99.1 us -> 88.1 us (0.89)
  Pallas kernels: 98.4 us -> 87.3 us
    pallas_call x1, Pallas kernels: 95.3 us -> 84.3 us  [on_device(): pl.pallas_call(body, out_shape=(jax.ShapeDtypeStruct((HALF, 128), BF), ja...]
where the time goes in v4:
time: 88.1 us; the launch traced here: 87.9 us
  Pallas kernels  87.3 us (99%)
    pallas_call x1, Pallas kernels, on_device(): pl.pallas_call(body, out_shape=(jax.ShapeDtypeStruct((HALF, 128), BF), ja...  84.3 us
    pallas_call x1, Pallas kernels, on_device(): pl.pallas_call(finish, out_shape=(jax.ShapeDtypeStruct((HALF, 128), BF),...  3.03 us

profile of v4, /device:TPU:1, one launch (start us, length us, event | category | flops | bytes accessed | tf_op | source)
XLA Modules:
  0.0 87.9 jit_solution(17386030305275733450)
XLA Ops:
  0.6 84.3 %backward.1 = (bf16[1280,128]{1,0:T(8,128)(2,1)}, bf16[6,4,64,256]{3,2,1,0:T(8,128)(2,1)}, bf16[4,32,1536]{2,1,0:T(8,128)(2,1)}, f32[1,256]{1,0:T(1,128)}, f32[1,1536]{1,0:T(1,128)}) custom-call(bf16[1280,128]{1,0:T(8,128)(2,1)} %x_hbm.1, bf16[1280,128]{1,0:T(8,128)(2,1)} %cot_hbm.1, bf16[2560,1536]{1,0:T(8,128)(2,1)} %gate_hbm.1, ...), custom_call_target="tpu_custom_call" | custom-call | tf_op jit(solution)/shard_map/backward/pallas_call | solution.py:588
  84.9 3.0 %outputs.1 = (bf16[1280,128]{1,0:T(8,128)(2,1)}, f32[128,1536]{1,0:T(8,128)}, f32[128,1536]{1,0:T(8,128)}, f32[1536,128]{1,0:T(8,128)}, f32[128]{0:T(128)}, /*index=5*/f32[128]{0:T(128)}, f32[1536]{0:T(1024)}) custom-call(bf16[1280,128]{1,0:T(8,128)(2,1)} %get-tuple-element.12.ig, bf16[6,4,64,256]{3,2,1,0:T(8,128)(2,1)} %get-tuple-element.13.ag, ...), custom_call_target="tpu_custom_call" | custom-call | tf_op jit(solution)/shard_map/outputs/pallas_call | solution.py:647

commit v5 on v4

--- a/solution.py
+++ b/solution.py
@@ -27,8 +27,8 @@
 
 def body(
     x_hbm, cot_hbm, gate_hbm, up_hbm, gw_hbm, uw_hbm, dw_hbm,
-    ig_out, ag, dag, sq_out, dsq_out,
-    allb, aa, cc, gbuf, ubuf, hid, xb, xt, dgt, ig, gw, uw,
+    ig_hbm, ag_hbm, dag_hbm, sq_hbm, dsq_hbm,
+    sq_out, dsq_out, ig_out, ag, dag, out_sem, allb, aa, cc, gbuf, ubuf, hid, xb, xt, dgt, ig, gw, uw,
     wt, gacc, gs, rs, ds, dr, igs, igr, sqacc, sqs, sqr, dsqs, dsqr,
     send_sem, recv_sem, x_send, x_recv, d2d_send, d2d_recv, loc_sem, tile_sem,
     rs_send, rs_recv, ag_send, ag_recv, q_send, q_recv, r_send, r_recv,
@@ -83,14 +83,14 @@
     own_uw.start()
 
     barrier = pltpu.get_barrier_semaphore()
-    for d in range(1, 16):
-        pl.semaphore_signal(barrier, inc=1, device_id={"tp": (tp + d) % 16}, device_id_type=MESH)
+    for d in ((0, 1), (0, -1), (1, 0), (-1, 0)):
+        pl.semaphore_signal(barrier, inc=1, device_id={"tp": blk(*d)}, device_id_type=MESH)
     for d in range(1, 4):
         peer = (rep + d) % 4
         pl.semaphore_signal(barrier, inc=1, device_id={"rep": peer}, device_id_type=MESH)
         pl.semaphore_signal(barrier, inc=1, device_id={"rep": peer, "fs": sib}, device_id_type=MESH)
     pl.semaphore_signal(barrier, inc=1, device_id={"fs": sib}, device_id_type=MESH)
-    pl.semaphore_wait(barrier, 22)
+    pl.semaphore_wait(barrier, 11)
 
     def row0(p):
         w = (p + 11) // 16
@@ -211,6 +211,42 @@
             device_id={"fs": sib},
             device_id_type=MESH,
         )
+
+    def tile(i):
+        slot = i % 2
+        r = tile_rows(i)
+        for c in loads(i):
+            c.wait()
+
+        def sub(k, carry):
+            q = pl.multiple_of(k * 32, 32)
+            for j in range(NCH):
+                g = gbuf[slot, pl.ds(q, 32), j * CH : (j + 1) * CH].astype(F32)
+                u = ubuf[slot, pl.ds(q, 32), j * CH : (j + 1) * CH].astype(F32)
+                s = 1.0 / (1.0 + jnp.exp(-g))
+                a = g * s
+                hid[pl.ds(q, 32), j * CH : (j + 1) * CH] = (a * u).astype(BF)
+                aa[j, pl.ds(pl.multiple_of(r + q, 32), 32), :] = a.astype(BF)
+                cc[j, pl.ds(pl.multiple_of(r + q, 32), 32), :] = (
+                    u * s * (1.0 + g * (1.0 - s))
+                ).astype(BF)
+            return carry
+
+        lax.fori_loop(0, TP // 32, sub, 0)
+
+        @pl.when(i < 8)
+        def _():
+            for c in loads(i + 2):
+                c.start()
+
+        ct = allb[tp, pl.ds(r, TP), :].astype(F32).T.astype(BF)
+        dgt[...] += jnp.dot(ct, hid[...], preferred_element_type=F32)
+
+    def transpose_x(i, carry):
+        r = pl.multiple_of(i * 128, 128)
+        v = xb[pl.ds(r, 128), :].astype(F32)
+        xt[:, pl.ds(r, 128)] = v.T.astype(BF)
+        return carry
 
     for c in own_dw:
         c.wait()
@@ -229,59 +265,25 @@
     own_uw.wait()
     dgt[...] = jnp.zeros_like(dgt)
     sqacc[...] = jnp.zeros_like(sqacc)
+    tile(0)
     for h in shares:
         r1(h)
     r0(whole(2))
     r1(whole(0))
-    cot_pair.wait_recv()
-    x_pair.wait_recv()
-
-    def transpose_x(i, carry):
-        r = pl.multiple_of(i * 128, 128)
-        v = xb[pl.ds(r, 128), :].astype(F32)
-        xt[:, pl.ds(r, 128)] = v.T.astype(BF)
-        return carry
-
+    tile(1)
     for h in shares:
         r2(h)
     for h in shares:
         r3(h)
     r0(whole(3))
     r1(whole(1))
+    cot_pair.wait_recv()
+    x_pair.wait_recv()
     lax.fori_loop(0, TOK // 128, transpose_x, 0)
     for h in shares:
         r4(h)
     r0(whole(4))
-
-    def tile(i):
-        slot = i % 2
-        r = tile_rows(i)
-        for c in loads(i):
-            c.wait()
-
-        def sub(k, carry):
-            q = pl.multiple_of(k * 32, 32)
-            for j in range(NCH):
-                g = gbuf[slot, pl.ds(q, 32), j * CH : (j + 1) * CH].astype(F32)
-                u = ubuf[slot, pl.ds(q, 32), j * CH : (j + 1) * CH].astype(F32)
-                s = 1.0 / (1.0 + jnp.exp(-g))
-                a = g * s
-                hid[pl.ds(q, 32), j * CH : (j + 1) * CH] = (a * u).astype(BF)
-                aa[j, pl.ds(pl.multiple_of(r + q, 32), 32), :] = a.astype(BF)
-                cc[j, pl.ds(pl.multiple_of(r + q, 32), 32), :] = (
-                    u * s * (1.0 + g * (1.0 - s))
-                ).astype(BF)
-            return carry
-
-        lax.fori_loop(0, TP // 32, sub, 0)
-
-        @pl.when(i < 8)
-        def _():
-            for c in loads(i + 2):
-                c.start()
-
-        ct = allb[tp, pl.ds(r, TP), :].astype(F32).T.astype(BF)
-        dgt[...] += jnp.dot(ct, hid[...], preferred_element_type=F32)
+    tile(2)
 
     def first(k, carry):
         r2(whole(k))
@@ -290,7 +292,7 @@
         def _():
             r1(whole(k + 2))
 
-        tile(2 * k)
+        tile(k + 3 + k // 3)
 
         @pl.when(k == 0)
         def _():
@@ -305,10 +307,9 @@
         def _():
             r4(whole(k - 1))
 
-        tile(2 * k + 1)
-
         @pl.when(k >= 2)
         def _():
+            tile(2 * k + 2)
             r5(whole(k - 2))
             to_sibling(k - 2, FAR)
 
@@ -317,7 +318,7 @@
     lax.fori_loop(0, NCOT - 1, first, 0)
 
     def scatter(src, dst, s_sem, r_sem):
-        for d in range(1, 4):
+        for d in (2, 1, 3):
             peer = (rep + d) % 4
             pltpu.make_async_remote_copy(
                 src_ref=src.at[peer],
@@ -329,7 +330,7 @@
             ).start()
 
     def spread(buf, s_sem, r_sem):
-        for d in range(1, 4):
+        for d in (2, 1, 3):
             pltpu.make_async_remote_copy(
                 src_ref=buf.at[rep],
                 dst_ref=buf.at[rep],
@@ -345,26 +346,25 @@
 
     k = NCOT - 1
     r2(whole(k))
-    tile(2 * k)
+    tile(9)
     r3(whole(k))
     to_sibling(k, NEAR)
     r4(whole(k - 1))
     r0(whole(k + 1))
-    tile(2 * k + 1)
     r5(whole(k - 2))
     to_sibling(k - 2, FAR)
-    for j in range(4):
-        ds[j] = (dgt[32 * j : 32 * j + 32, :] * scale).astype(BF)
-    dr[rep] = ds[rep]
     r4(whole(k))
     r5(whole(k - 1))
     to_sibling(k - 1, FAR)
     r0(whole(k + 2))
     r1(whole(k + 1))
-    scatter(ds, dr, rs_send.at[NCH], rs_recv.at[NCH])
     r5(whole(k))
     to_sibling(k, FAR)
     r0(whole(k + 3))
+    for j in range(4):
+        ds[j] = (dgt[32 * j : 32 * j + 32, :] * scale).astype(BF)
+    dr[rep] = ds[rep]
+    scatter(ds, dr, rs_send.at[NCH], rs_recv.at[NCH])
     take(x_recv.at[0], 12)
     for k in range(NCOT):
         take(d2d_recv.at[k], 15)
@@ -375,8 +375,8 @@
             wt[128 * k : 128 * k + 128, :] = allb[k, fr, :].astype(F32).T.astype(BF)
 
     def main_tile(c, j):
-        for i in range(2):
-            rows = pl.ds(j * TM + i * (TM // 2), TM // 2)
+        for i in range(4):
+            rows = pl.ds(j * 2 * TM + i * (TM // 2), TM // 2)
             lhs = jnp.concatenate([allb[k, rows, :] for k in range(16)], axis=1)
             hg = jnp.dot(lhs, wt[...], preferred_element_type=F32)
             cc[c, rows, :] = (hg * cc[c, rows, :].astype(F32)).astype(BF)
@@ -454,42 +454,46 @@
         def _():
             take(x_recv.at[1], 12)
 
+        @pl.when(c >= 1)
+        def _():
+            @pl.when(k - 1 < NPAY)
+            def _():
+                r4(whole(k - 1))
+
+            @pl.when(k < NPAY)
+            def _():
+                r2(whole(k))
+
+            @pl.when(k + 1 < NPAY)
+            def _():
+                r1(whole(k + 1))
+
         main_weight(c)
         main_tile(c, 0)
 
-        @pl.when((c >= 1) & (k - 1 < NPAY))
-        def _():
-            r4(whole(k - 1))
-
         @pl.when(c == 0)
         def _():
+            r2(whole(NCOT))
+            r1(whole(NCOT + 1))
             r0(whole(NPAY - 1))
 
+        @pl.when((c >= 1) & (k < NPAY))
+        def _():
+            r3(whole(k))
+
+        @pl.when(c == 2)
+        def _():
+            reduce_down()
+
+        @pl.when(c == 4)
+        def _():
+            finish_down()
+
         main_tile(c, 1)
 
-        @pl.when(k < NPAY)
-        def _():
-            r2(whole(k))
-
-        @pl.when(k + 1 < NPAY)
-        def _():
-            r1(whole(k + 1))
-
-        main_tile(c, 2)
-
-        @pl.when(k < NPAY)
-        def _():
-            r3(whole(k))
-
-        @pl.when(c == 2)
-        def _():
-            reduce_down()
-
-        @pl.when(c == 4)
-        def _():
-            finish_down()
-
-        main_tile(c, 3)
+        @pl.when(c == 0)
+        def _():
+            r3(whole(NCOT))
 
         @pl.when(c == 4)
         def _():
@@ -526,16 +530,29 @@
             device_id=other,
             device_id_type=MESH,
         ).start()
+    leave = [pltpu.make_async_copy(ag.at[k], ag_hbm.at[k], out_sem.at[k]) for k in range(NCH)]
+    leave.append(pltpu.make_async_copy(dag, dag_hbm, out_sem.at[NCH]))
+    leave.append(pltpu.make_async_copy(ig_out, ig_hbm, out_sem.at[NCH + 1]))
+    leave[NCH].start()
+    for k in range(NCH - 2):
+        three(ag.at[k], ag_recv.at[k])
+        leave[k].start()
     for i, v in enumerate(input_part(mine)):
         ig[i * TM : (i + 1) * TM, :] = v.astype(BF).astype(F32)
     ig_pair.wait_recv()
     ig_out[...] = (ig[...] + igr[...].astype(F32)).astype(BF)
+    three(ag.at[NCH - 2], ag_recv.at[NCH - 2])
+    leave[NCH - 2].start()
+    leave[NCH + 1].start()
     all15 = dsqr.at[pl.ds(0, 15)]
     pltpu.make_async_copy(all15, all15, q_recv).wait()
     total = dsqr[0]
     for k in range(1, 16):
         total = total + dsqr[k]
     dsq_out[...] = total
+    leave.append(pltpu.make_async_copy(dsq_out, dsq_hbm, out_sem.at[NCH + 2]))
+    leave.append(pltpu.make_async_copy(sq_out, sq_hbm, out_sem.at[NCH + 3]))
+    leave[NCH + 2].start()
 
     for p in range(NPAY):
         take(send_sem.at[p], 15)
@@ -553,8 +570,8 @@
     cot_pair.wait_send()
     x_pair.wait_send()
     ig_pair.wait_send()
-    for k in range(NCH):
-        three(ag.at[k], ag_recv.at[k])
+    three(ag.at[NCH - 1], ag_recv.at[NCH - 1])
+    leave[NCH - 1].start()
     all7 = sqr.at[pl.ds(0, 7)]
     pltpu.make_async_copy(all7, all7, r_send.at[3]).wait()
     pltpu.make_async_copy(all7, all7, r_recv.at[3]).wait()
@@ -562,6 +579,9 @@
     for k in range(1, 8):
         total = total + sqr[k]
     sq_out[...] = total
+    leave[NCH + 3].start()
+    for c in leave:
+        c.wait()
 
 
 def finish(ig, ag, dag, sq, dsq, ig_out, gg_out, ug_out, dg_out, gsq_out, usq_out, dsq_out):
@@ -595,8 +615,14 @@
             jax.ShapeDtypeStruct((1, FH), F32),
         ),
         in_specs=[anyspec] * 7,
-        out_specs=(vm,) * 5,
+        out_specs=(anyspec,) * 5,
         scratch_shapes=[
+            pltpu.VMEM((1, 256), F32),
+            pltpu.VMEM((1, FH), F32),
+            pltpu.VMEM((HALF, 128), BF),
+            pltpu.VMEM((NCH, 4, 64, CH), BF),
+            pltpu.VMEM((4, 32, FH), BF),
+            dma((NCH + 4,)),
             pltpu.VMEM((16, TOK + FH, 128), BF),
             pltpu.VMEM((NCH, TOK, CH), BF),
             pltpu.VMEM((NCH, TOK, CH), BF),

time: 88.1 us -> 85.8 us (0.974)
  Pallas kernels: 87.3 us -> 85.1 us
    pallas_call x1, Pallas kernels: 84.3 us -> 82 us  [on_device(): pl.pallas_call(body, out_shape=(jax.ShapeDtypeStruct((HALF, 128), BF), ja...]
where the time goes in v5:
time: 85.8 us; the launch traced here: 85.7 us
  Pallas kernels  85.1 us (99%)
    pallas_call x1, Pallas kernels, on_device(): pl.pallas_call(body, out_shape=(jax.ShapeDtypeStruct((HALF, 128), BF), ja...  82 us
    pallas_call x1, Pallas kernels, on_device(): pl.pallas_call(finish, out_shape=(jax.ShapeDtypeStruct((HALF, 128), BF),...  3.03 us

profile of v5, /device:TPU:1, one launch (start us, length us, event | category | flops | bytes accessed | tf_op | source)
XLA Modules:
  0.0 85.7 jit_solution(6078430992672959066)
XLA Ops:
  0.6 82.0 %backward.1 = (bf16[1280,128]{1,0:T(8,128)(2,1)}, bf16[6,4,64,256]{3,2,1,0:T(8,128)(2,1)}, bf16[4,32,1536]{2,1,0:T(8,128)(2,1)}, f32[1,256]{1,0:T(1,128)}, f32[1,1536]{1,0:T(1,128)}) custom-call(bf16[1280,128]{1,0:T(8,128)(2,1)} %x_hbm.1, bf16[1280,128]{1,0:T(8,128)(2,1)} %cot_hbm.1, bf16[2560,1536]{1,0:T(8,128)(2,1)} %gate_hbm.1, ...), custom_call_target="tpu_custom_call" | custom-call | tf_op jit(solution)/shard_map/backward/pallas_call | solution.py:608
  82.7 3.0 %outputs.1 = (bf16[1280,128]{1,0:T(8,128)(2,1)}, f32[128,1536]{1,0:T(8,128)}, f32[128,1536]{1,0:T(8,128)}, f32[1536,128]{1,0:T(8,128)}, f32[128]{0:T(128)}, /*index=5*/f32[128]{0:T(128)}, f32[1536]{0:T(1024)}) custom-call(bf16[1280,128]{1,0:T(8,128)(2,1)} %get-tuple-element.12.ig, bf16[6,4,64,256]{3,2,1,0:T(8,128)(2,1)} %get-tuple-element.13.ag, ...), custom_call_target="tpu_custom_call" | custom-call | tf_op jit(solution)/shard_map/outputs/pallas_call | solution.py:673

commit v6 on v5

--- a/solution.py
+++ b/solution.py
@@ -29,7 +29,7 @@
     x_hbm, cot_hbm, gate_hbm, up_hbm, gw_hbm, uw_hbm, dw_hbm,
     ig_hbm, ag_hbm, dag_hbm, sq_hbm, dsq_hbm,
     sq_out, dsq_out, ig_out, ag, dag, out_sem, allb, aa, cc, gbuf, ubuf, hid, xb, xt, dgt, ig, gw, uw,
-    wt, gacc, gs, rs, ds, dr, igs, igr, sqacc, sqs, sqr, dsqs, dsqr,
+    gacc, gs, rs, ds, dr, igs, igr, sqacc, sqs, sqr, dsqs, dsqr,
     send_sem, recv_sem, x_send, x_recv, d2d_send, d2d_recv, loc_sem, tile_sem,
     rs_send, rs_recv, ag_send, ag_recv, q_send, q_recv, r_send, r_recv,
 ):
@@ -88,9 +88,8 @@
     for d in range(1, 4):
         peer = (rep + d) % 4
         pl.semaphore_signal(barrier, inc=1, device_id={"rep": peer}, device_id_type=MESH)
-        pl.semaphore_signal(barrier, inc=1, device_id={"rep": peer, "fs": sib}, device_id_type=MESH)
     pl.semaphore_signal(barrier, inc=1, device_id={"fs": sib}, device_id_type=MESH)
-    pl.semaphore_wait(barrier, 11)
+    pl.semaphore_wait(barrier, 8)
 
     def row0(p):
         w = (p + 11) // 16
@@ -369,16 +368,15 @@
     for k in range(NCOT):
         take(d2d_recv.at[k], 15)
 
-    def main_weight(c):
+    def main_tile(c, j):
         fr = pl.ds(pl.multiple_of(TOK + c * CH, CH), CH)
-        for k in range(16):
-            wt[128 * k : 128 * k + 128, :] = allb[k, fr, :].astype(F32).T.astype(BF)
-
-    def main_tile(c, j):
         for i in range(4):
             rows = pl.ds(j * 2 * TM + i * (TM // 2), TM // 2)
             lhs = jnp.concatenate([allb[k, rows, :] for k in range(16)], axis=1)
-            hg = jnp.dot(lhs, wt[...], preferred_element_type=F32)
+            rhs = jnp.concatenate([allb[k, fr, :] for k in range(16)], axis=1)
+            hg = lax.dot_general(
+                lhs, rhs, (((1,), (1,)), ((), ())), preferred_element_type=F32
+            )
             cc[c, rows, :] = (hg * cc[c, rows, :].astype(F32)).astype(BF)
             aa[c, rows, :] = (hg * aa[c, rows, :].astype(F32)).astype(BF)
 
@@ -416,6 +414,7 @@
         w = w[:, 0:128] + w[:, 128:256]
         sqacc[pl.ds(pl.multiple_of(32 * rep, 32), 32), :] += w[0:32]
         sqacc[pl.ds(pl.multiple_of(128 + 32 * rep, 32), 32), :] += w[32:64]
+    def spread_grads(c):
         spread(ag.at[c], ag_send.at[c], ag_recv.at[c])
 
     def reduce_down():
@@ -468,7 +467,6 @@
             def _():
                 r1(whole(k + 1))
 
-        main_weight(c)
         main_tile(c, 0)
 
         @pl.when(c == 0)
@@ -502,6 +500,7 @@
         @pl.when(c >= 2)
         def _():
             reduce_grads(c - 2)
+            spread_grads(c - 2)
 
         @pl.when((c >= 1) & (k - 1 < NPAY))
         def _():
@@ -514,10 +513,10 @@
     lax.fori_loop(0, NCH, chunk, 0)
 
     reduce_grads(NCH - 2)
+    spread_grads(NCH - 2)
     for i, v in enumerate(input_part(theirs)):
         igs[i * TM : (i + 1) * TM, :] = v.astype(BF)
     reduce_grads(NCH - 1)
-    ig_pair.start()
     sqs[...] = jnp.sum(sqacc[...].T, axis=0, keepdims=True)
     sqr[rep * 2 + fs] = sqs[...]
     for d in range(1, 8):
@@ -530,6 +529,8 @@
             device_id=other,
             device_id_type=MESH,
         ).start()
+    spread_grads(NCH - 1)
+    ig_pair.start()
     leave = [pltpu.make_async_copy(ag.at[k], ag_hbm.at[k], out_sem.at[k]) for k in range(NCH)]
     leave.append(pltpu.make_async_copy(dag, dag_hbm, out_sem.at[NCH]))
     leave.append(pltpu.make_async_copy(ig_out, ig_hbm, out_sem.at[NCH + 1]))
@@ -635,7 +636,6 @@
             pltpu.VMEM((HALF, 128), F32),
             pltpu.VMEM((128, FH), BF),
             pltpu.VMEM((128, FH), BF),
-            pltpu.VMEM((2048, CH), BF),
             pltpu.VMEM((128, 2 * CH), F32),
             pltpu.VMEM((NCH, 4, 64, CH), BF),
             pltpu.VMEM((NCH, 4, 64, CH), BF),

time: 85.8 us -> 85.1 us (level)
  no operation moved by 1% of the time
where the time goes in v6:
time: 85.1 us; the launch traced here: 85 us
  Pallas kernels  84.3 us (99%)
    pallas_call x1, Pallas kernels, on_device(): pl.pallas_call(body, out_shape=(jax.ShapeDtypeStruct((HALF, 128), BF), ja...  81.3 us
    pallas_call x1, Pallas kernels, on_device(): pl.pallas_call(finish, out_shape=(jax.ShapeDtypeStruct((HALF, 128), BF),...  3.03 us

profile of v6, /device:TPU:1, one launch (start us, length us, event | category | flops | bytes accessed | tf_op | source)
XLA Modules:
  0.0 85.0 jit_solution(3192449969466580875)
XLA Ops:
  0.6 81.3 %backward.1 = (bf16[1280,128]{1,0:T(8,128)(2,1)}, bf16[6,4,64,256]{3,2,1,0:T(8,128)(2,1)}, bf16[4,32,1536]{2,1,0:T(8,128)(2,1)}, f32[1,256]{1,0:T(1,128)}, f32[1,1536]{1,0:T(1,128)}) custom-call(bf16[1280,128]{1,0:T(8,128)(2,1)} %x_hbm.1, bf16[1280,128]{1,0:T(8,128)(2,1)} %cot_hbm.1, bf16[2560,1536]{1,0:T(8,128)(2,1)} %gate_hbm.1, ...), custom_call_target="tpu_custom_call" | custom-call | tf_op jit(solution)/shard_map/backward/pallas_call | solution.py:609
  82.0 3.0 %outputs.1 = (bf16[1280,128]{1,0:T(8,128)(2,1)}, f32[128,1536]{1,0:T(8,128)}, f32[128,1536]{1,0:T(8,128)}, f32[1536,128]{1,0:T(8,128)}, f32[128]{0:T(128)}, /*index=5*/f32[128]{0:T(128)}, f32[1536]{0:T(1024)}) custom-call(bf16[1280,128]{1,0:T(8,128)(2,1)} %get-tuple-element.12.ig, bf16[6,4,64,256]{3,2,1,0:T(8,128)(2,1)} %get-tuple-element.13.ag, ...), custom_call_target="tpu_custom_call" | custom-call | tf_op jit(solution)/shard_map/outputs/pallas_call | solution.py:673

commit v7 on v6

--- a/solution.py
+++ b/solution.py
@@ -22,6 +22,7 @@
 NXC = 2
 NPAY = NCOT + NCH - NXC
 TM = 640
+TS = 640
 TP = 256
 
 
@@ -348,30 +349,29 @@
     tile(9)
     r3(whole(k))
     to_sibling(k, NEAR)
+    r0(whole(k + 1))
     r4(whole(k - 1))
-    r0(whole(k + 1))
     r5(whole(k - 2))
     to_sibling(k - 2, FAR)
     r4(whole(k))
+    r1(whole(k + 1))
+    r0(whole(k + 2))
     r5(whole(k - 1))
     to_sibling(k - 1, FAR)
-    r0(whole(k + 2))
-    r1(whole(k + 1))
     r5(whole(k))
     to_sibling(k, FAR)
     r0(whole(k + 3))
     for j in range(4):
         ds[j] = (dgt[32 * j : 32 * j + 32, :] * scale).astype(BF)
     dr[rep] = ds[rep]
-    scatter(ds, dr, rs_send.at[NCH], rs_recv.at[NCH])
     take(x_recv.at[0], 12)
     for k in range(NCOT):
         take(d2d_recv.at[k], 15)
 
-    def main_tile(c, j):
+    def main_tile(c):
         fr = pl.ds(pl.multiple_of(TOK + c * CH, CH), CH)
-        for i in range(4):
-            rows = pl.ds(j * 2 * TM + i * (TM // 2), TM // 2)
+        for i in range(TOK // TS):
+            rows = pl.ds(i * TS, TS)
             lhs = jnp.concatenate([allb[k, rows, :] for k in range(16)], axis=1)
             rhs = jnp.concatenate([allb[k, fr, :] for k in range(16)], axis=1)
             hg = lax.dot_general(
@@ -452,49 +452,40 @@
         @pl.when(c == 1)
         def _():
             take(x_recv.at[1], 12)
-
-        @pl.when(c >= 1)
-        def _():
-            @pl.when(k - 1 < NPAY)
-            def _():
-                r4(whole(k - 1))
-
-            @pl.when(k < NPAY)
+            scatter(ds, dr, rs_send.at[NCH], rs_recv.at[NCH])
+
+        @pl.when((c >= 1) & (k - 1 < NPAY))
+        def _():
+            r4(whole(k - 1))
+
+        def rounds(turn):
+            @pl.when((k < NPAY) & turn)
             def _():
                 r2(whole(k))
 
-            @pl.when(k + 1 < NPAY)
-            def _():
-                r1(whole(k + 1))
-
-        main_tile(c, 0)
-
-        @pl.when(c == 0)
-        def _():
-            r2(whole(NCOT))
-            r1(whole(NCOT + 1))
-            r0(whole(NPAY - 1))
-
-        @pl.when((c >= 1) & (k < NPAY))
+                @pl.when(k + 1 < NPAY)
+                def _():
+                    r1(whole(k + 1))
+
+                @pl.when(c == 0)
+                def _():
+                    r0(whole(NPAY - 1))
+
+        rounds((c >= 1) | (fs == 1))
+        main_tile(c)
+        rounds((c == 0) & (fs == 0))
+
+        @pl.when(k < NPAY)
         def _():
             r3(whole(k))
 
-        @pl.when(c == 2)
+        @pl.when(c == 3)
         def _():
             reduce_down()
 
-        @pl.when(c == 4)
+        @pl.when(c == 5)
         def _():
             finish_down()
-
-        main_tile(c, 1)
-
-        @pl.when(c == 0)
-        def _():
-            r3(whole(NCOT))
-
-        @pl.when(c == 4)
-        def _():
             send_down_sq()
 
         @pl.when(c >= 2)
@@ -512,10 +503,11 @@
 
     lax.fori_loop(0, NCH, chunk, 0)
 
+    for i, v in enumerate(input_part(theirs)):
+        igs[i * TM : (i + 1) * TM, :] = v.astype(BF)
     reduce_grads(NCH - 2)
     spread_grads(NCH - 2)
-    for i, v in enumerate(input_part(theirs)):
-        igs[i * TM : (i + 1) * TM, :] = v.astype(BF)
+    ig_pair.start()
     reduce_grads(NCH - 1)
     sqs[...] = jnp.sum(sqacc[...].T, axis=0, keepdims=True)
     sqr[rep * 2 + fs] = sqs[...]
@@ -530,7 +522,6 @@
             device_id_type=MESH,
         ).start()
     spread_grads(NCH - 1)
-    ig_pair.start()
     leave = [pltpu.make_async_copy(ag.at[k], ag_hbm.at[k], out_sem.at[k]) for k in range(NCH)]
     leave.append(pltpu.make_async_copy(dag, dag_hbm, out_sem.at[NCH]))
     leave.append(pltpu.make_async_copy(ig_out, ig_hbm, out_sem.at[NCH + 1]))

time: 85.1 us -> 85.6 us (level)
  no operation moved by 1% of the time
where the time goes in v7:
time: 85.6 us; the launch traced here: 85.4 us
  Pallas kernels  84.8 us (99%)
    pallas_call x1, Pallas kernels, on_device(): pl.pallas_call(body, out_shape=(jax.ShapeDtypeStruct((HALF, 128), BF), ja...  81.8 us
    pallas_call x1, Pallas kernels, on_device(): pl.pallas_call(finish, out_shape=(jax.ShapeDtypeStruct((HALF, 128), BF),...  3.03 us

profile of v7, /device:TPU:1, one launch (start us, length us, event | category | flops | bytes accessed | tf_op | source)
XLA Modules:
  0.0 85.4 jit_solution(9029752314888852457)
XLA Ops:
  0.6 81.8 %backward.1 = (bf16[1280,128]{1,0:T(8,128)(2,1)}, bf16[6,4,64,256]{3,2,1,0:T(8,128)(2,1)}, bf16[4,32,1536]{2,1,0:T(8,128)(2,1)}, f32[1,256]{1,0:T(1,128)}, f32[1,1536]{1,0:T(1,128)}) custom-call(bf16[1280,128]{1,0:T(8,128)(2,1)} %x_hbm.1, bf16[1280,128]{1,0:T(8,128)(2,1)} %cot_hbm.1, bf16[2560,1536]{1,0:T(8,128)(2,1)} %gate_hbm.1, ...), custom_call_target="tpu_custom_call" | custom-call | tf_op jit(solution)/shard_map/backward/pallas_call | solution.py:600
  82.4 3.0 %outputs.1 = (bf16[1280,128]{1,0:T(8,128)(2,1)}, f32[128,1536]{1,0:T(8,128)}, f32[128,1536]{1,0:T(8,128)}, f32[1536,128]{1,0:T(8,128)}, f32[128]{0:T(128)}, /*index=5*/f32[128]{0:T(128)}, f32[1536]{0:T(1024)}) custom-call(bf16[1280,128]{1,0:T(8,128)(2,1)} %get-tuple-element.12.ig, bf16[6,4,64,256]{3,2,1,0:T(8,128)(2,1)} %get-tuple-element.13.ag, ...), custom_call_target="tpu_custom_call" | custom-call | tf_op jit(solution)/shard_map/outputs/pallas_call | solution.py:664

commit v8 on v7

--- a/solution.py
+++ b/solution.py
@@ -458,22 +458,19 @@
         def _():
             r4(whole(k - 1))
 
-        def rounds(turn):
-            @pl.when((k < NPAY) & turn)
-            def _():
-                r2(whole(k))
-
-                @pl.when(k + 1 < NPAY)
-                def _():
-                    r1(whole(k + 1))
-
-                @pl.when(c == 0)
-                def _():
-                    r0(whole(NPAY - 1))
-
-        rounds((c >= 1) | (fs == 1))
+        @pl.when(k < NPAY)
+        def _():
+            r2(whole(k))
+
+        @pl.when(k + 1 < NPAY)
+        def _():
+            r1(whole(k + 1))
+
+        @pl.when(c == 0)
+        def _():
+            r0(whole(NPAY - 1))
+
         main_tile(c)
-        rounds((c == 0) & (fs == 0))
 
         @pl.when(k < NPAY)
         def _():

time: 85.6 us -> 85.1 us (level)
  no operation moved by 1% of the time
where the time goes in v8:
time: 85.1 us; the launch traced here: 84.9 us
  Pallas kernels  84.3 us (99%)
    pallas_call x1, Pallas kernels, on_device(): pl.pallas_call(body, out_shape=(jax.ShapeDtypeStruct((HALF, 128), BF), ja...  81.3 us
    pallas_call x1, Pallas kernels, on_device(): pl.pallas_call(finish, out_shape=(jax.ShapeDtypeStruct((HALF, 128), BF),...  3.03 us

profile of v8, /device:TPU:1, one launch (start us, length us, event | category | flops | bytes accessed | tf_op | source)
XLA Modules:
  0.0 84.9 jit_solution(2445054023458947886)
XLA Ops:
  0.6 81.3 %backward.1 = (bf16[1280,128]{1,0:T(8,128)(2,1)}, bf16[6,4,64,256]{3,2,1,0:T(8,128)(2,1)}, bf16[4,32,1536]{2,1,0:T(8,128)(2,1)}, f32[1,256]{1,0:T(1,128)}, f32[1,1536]{1,0:T(1,128)}) custom-call(bf16[1280,128]{1,0:T(8,128)(2,1)} %x_hbm.1, bf16[1280,128]{1,0:T(8,128)(2,1)} %cot_hbm.1, bf16[2560,1536]{1,0:T(8,128)(2,1)} %gate_hbm.1, ...), custom_call_target="tpu_custom_call" | custom-call | tf_op jit(solution)/shard_map/backward/pallas_call | solution.py:597
  81.9 3.0 %outputs.1 = (bf16[1280,128]{1,0:T(8,128)(2,1)}, f32[128,1536]{1,0:T(8,128)}, f32[128,1536]{1,0:T(8,128)}, f32[1536,128]{1,0:T(8,128)}, f32[128]{0:T(128)}, /*index=5*/f32[128]{0:T(128)}, f32[1536]{0:T(1024)}) custom-call(bf16[1280,128]{1,0:T(8,128)(2,1)} %get-tuple-element.12.ig, bf16[6,4,64,256]{3,2,1,0:T(8,128)(2,1)} %get-tuple-element.13.ag, ...), custom_call_target="tpu_custom_call" | custom-call | tf_op jit(solution)/shard_map/outputs/pallas_call | solution.py:661

commit v9 on v8

--- a/solution.py
+++ b/solution.py
@@ -354,10 +354,10 @@
     r5(whole(k - 2))
     to_sibling(k - 2, FAR)
     r4(whole(k))
+    r5(whole(k - 1))
+    to_sibling(k - 1, FAR)
     r1(whole(k + 1))
     r0(whole(k + 2))
-    r5(whole(k - 1))
-    to_sibling(k - 1, FAR)
     r5(whole(k))
     to_sibling(k, FAR)
     r0(whole(k + 3))

time: 85.1 us -> 85.3 us (level)
  no operation moved by 1% of the time
where the time goes in v9:
time: 85.3 us; the launch traced here: 85.1 us
  Pallas kernels  84.5 us (99%)
    pallas_call x1, Pallas kernels, on_device(): pl.pallas_call(body, out_shape=(jax.ShapeDtypeStruct((HALF, 128), BF), ja...  81.5 us
    pallas_call x1, Pallas kernels, on_device(): pl.pallas_call(finish, out_shape=(jax.ShapeDtypeStruct((HALF, 128), BF),...  3.03 us

profile of v9, /device:TPU:1, one launch (start us, length us, event | category | flops | bytes accessed | tf_op | source)
XLA Modules:
  0.0 85.1 jit_solution(9257887561773328369)
XLA Ops:
  0.6 81.5 %backward.1 = (bf16[1280,128]{1,0:T(8,128)(2,1)}, bf16[6,4,64,256]{3,2,1,0:T(8,128)(2,1)}, bf16[4,32,1536]{2,1,0:T(8,128)(2,1)}, f32[1,256]{1,0:T(1,128)}, f32[1,1536]{1,0:T(1,128)}) custom-call(bf16[1280,128]{1,0:T(8,128)(2,1)} %x_hbm.1, bf16[1280,128]{1,0:T(8,128)(2,1)} %cot_hbm.1, bf16[2560,1536]{1,0:T(8,128)(2,1)} %gate_hbm.1, ...), custom_call_target="tpu_custom_call" | custom-call | tf_op jit(solution)/shard_map/backward/pallas_call | solution.py:597
  82.1 3.0 %outputs.1 = (bf16[1280,128]{1,0:T(8,128)(2,1)}, f32[128,1536]{1,0:T(8,128)}, f32[128,1536]{1,0:T(8,128)}, f32[1536,128]{1,0:T(8,128)}, f32[128]{0:T(128)}, /*index=5*/f32[128]{0:T(128)}, f32[1536]{0:T(1024)}) custom-call(bf16[1280,128]{1,0:T(8,128)(2,1)} %get-tuple-element.12.ig, bf16[6,4,64,256]{3,2,1,0:T(8,128)(2,1)} %get-tuple-element.13.ag, ...), custom_call_target="tpu_custom_call" | custom-call | tf_op jit(solution)/shard_map/outputs/pallas_call | solution.py:661
